TPU v7x, 512 devices: a whole 4x8x8 slice. The times are simulated.
512 devices in a mesh: sp: 64 (over z, y), tp: 8 (over x, core).
Axes of the slice: x: 4, y: 8, z: 8, core: 2. Of those that a mesh axis runs over, the one named last changes fastest.
Arguments:
- tokens: bfloat16 [8192, 2048], P('sp', 'tp'), may hold values from -6 to 6
- pre_gain: float32 [2048], replicated, may hold values from 0.1 to 1.9
- w_query_stick: bfloat16 [2048, 1024], P(None, 'tp'), may hold values from -0.125 to 0.125
- w_key_stick: bfloat16 [2048, 1024], P(None, 'tp'), may hold values from -0.125 to 0.125
- w_value_stick: bfloat16 [2048, 1024], P(None, 'tp'), may hold values from -2 to 2, as said below
- w_query_window: bfloat16 [2048, 1024], P(None, 'tp'), may hold values from -20 to 20, as said below
- w_key_window: bfloat16 [2048, 512], P(None, 'tp'), may hold values from -1 to 1, as said below
- w_value_window: bfloat16 [2048, 512], P(None, 'tp'), may hold values from -2 to 2, as said below
- stick_bias: float32 [16], P('tp'), may hold values from -14 to -3
- sinks: float32 [16], P('tp'), may hold values from 2 to 6
- stick_gain: float32 [1024], P('tp'), may hold values from 0.1 to 1.9
- window_gain: float32 [1024], P('tp'), may hold values from 0.1 to 1.9
- w_out_stick: bfloat16 [1024, 2048], P('tp'), may hold values from -0.125 to 0.125
- w_out_window: bfloat16 [1024, 2048], P('tp'), may hold values from -0.125 to 0.125
- post_gain: float32 [2048], replicated, may hold values from 0.1 to 1.9
Outputs:
- layer_out: bfloat16 [8192, 2048], P(('sp', 'tp'))
Inputs may be any that keep to these rules, and one draw needn't show every extreme that they name: `w_key_window`: key weights of the windowed heads. `w_query_window`: query weights of the windowed heads. `w_value_stick`: value weights of the stick-breaking heads. `w_value_window`: value weights of the windowed heads.
All inputs are finite; a program needn't handle non-finite values.
Results may differ from a plain program's by a relative error of at most 0.018.
Values may be sent and summed in bfloat16 or wider, within the bound.
A program may use at most 64 MiB of HBM per device.

v0:
```python
import functools

import jax
import jax.numpy as jnp
from jax import lax
from jax.experimental import pallas as pl
from jax.experimental.pallas import tpu as pltpu
from jax.sharding import PartitionSpec as P

HEAD_DIM = 64
GROUP = 2
WINDOW = 128
EPS = 1e-06
LOG2E = 1.4426950408889634
MESH = pl.DeviceIdType.MESH


def dot(a, b):
    return jnp.dot(a, b, preferred_element_type=jnp.float32)


def dot_t(a, b):
    return lax.dot_general(a, b, (((1,), (1,)), ((), ())), preferred_element_type=jnp.float32)


def kernel(
    n_sp,
    tokens, pre_gain_in, wqs, wks, wvs, wqw, wkw, wvw, bias_in, sinks_in, sgain_in, wgain_in, wos, wow,
    post_gain_in, out,
    pre_gain, bias, sinks, sgain, wgain, post_gain, x, bias_buf, normed, vqs, vks, vvs, vqw, vkw, vvw, vos, vow,
    kv_send, kv_all, q_pad, staged,
    kvw, kvw_prev, w_out_buf, o_send, o_recv, s_out_buf,
    sq_send, sq_recv, total_w, comb, c_send, c_recv,
    w_sem, tok_sem, x_ss, x_rs, b_ss, b_rs, kv_ss, kv_rs, f_ss, f_rs,
    p_ss, p_rs, o_ss, o_rs, sq_ss, sq_rs, c_ss, c_rs,
):
    bf = jnp.bfloat16
    f32 = jnp.float32
    s = lax.axis_index("sp")
    t = lax.axis_index("tp")
    other = 1 - t
    rows, feat_half = tokens.shape
    feats = 2 * feat_half
    half = rows // 2
    quarter = half // 2
    hd = HEAD_DIM
    heads = wqs.shape[1] // hd
    kv_heads = wkw.shape[1] // hd
    sw = wqs.shape[1]

    barrier = pltpu.get_barrier_semaphore()
    me = s * 2 + t

    def greet(k, carry):
        peer = lax.rem(me + k, 2 * n_sp)
        pl.semaphore_signal(
            barrier, inc=1, device_id={"sp": peer // 2, "tp": lax.rem(peer, 2)}, device_id_type=MESH
        )
        return carry

    lax.fori_loop(1, 2 * n_sp, greet, 0)

    loads = [
        pltpu.make_async_copy(src, dst, w_sem.at[n])
        for n, (src, dst) in enumerate(
            [(wks, vks), (wvs, vvs), (wqs, vqs), (wkw, vkw), (wvw, vvw), (wqw, vqw), (wow, vow), (wos, vos),
             (bias_in, bias), (pre_gain_in, pre_gain), (sinks_in, sinks), (sgain_in, sgain),
             (wgain_in, wgain), (post_gain_in, post_gain)]
        )
    ]
    l_ks, l_vs, l_qs, l_kw, l_vw, l_qw, l_ow, l_os, l_bias, *l_small = loads
    tok_load = pltpu.make_async_copy(tokens, x.at[t], tok_sem)
    l_bias.start()
    tok_load.start()
    for load in l_small + loads[:8]:
        load.start()

    row_id = lax.broadcasted_iota(jnp.int32, (heads, 128), 0)
    bias_rows = jnp.zeros((heads, 128), f32)
    l_bias.wait()
    for i in range(heads):
        bias_rows = jnp.where(row_id == i, bias[i] * LOG2E, bias_rows)
    bias_buf[t] = bias_rows

    for load in l_small:
        load.wait()
    tok_load.wait()
    pl.semaphore_wait(barrier, 2 * n_sp - 1)

    def to_partner(src, dst, ss, rs):
        return pltpu.make_async_remote_copy(
            src_ref=src, dst_ref=dst, send_sem=ss, recv_sem=rs,
            device_id={"sp": s, "tp": other}, device_id_type=MESH,
        )

    x_copy = to_partner(x.at[t], x.at[t], x_ss, x_rs)
    b_copy = to_partner(bias_buf.at[t], bias_buf.at[t], b_ss, b_rs)
    x_copy.start()
    b_copy.start()
    x_copy.wait_recv()

    gain = pre_gain[...].reshape(1, feats)

    def norm_step(n, carry):
        part = pl.ds(pl.multiple_of(n * 32, 32), 32)
        left = x[0, part, :].astype(f32)
        right = x[1, part, :].astype(f32)
        stats = (
            jnp.sum(left * left, axis=1, keepdims=True) + jnp.sum(right * right, axis=1, keepdims=True)
        ) * (1.0 / feats)
        inv = lax.rsqrt(stats + EPS)
        normed[part, :feat_half] = (left * inv * gain[:, :feat_half]).astype(bf)
        normed[part, feat_half:] = (right * inv * gain[:, feat_half:]).astype(bf)
        return carry

    lax.fori_loop(0, rows // 32, norm_step, 0)

    l_ks.wait()
    keys = dot(normed[...], vks[...])
    l_vs.wait()
    values = dot(normed[...], vvs[...])
    for i in range(heads):
        cols = slice(i * hd, (i + 1) * hd)
        packed = jnp.concatenate([keys[:, cols], values[:, cols]], axis=1).astype(bf)
        kv_send[i, :, :half] = packed.reshape(2, half, 2 * hd)

    def scatter(send, slots, ss, rs):
        def step(k, carry):
            i = lax.rem(k // 2 + s, heads)
            u = lax.rem(k, 2)
            chip = t * heads + i
            is_self = jnp.logical_and(chip == s, u == t)

            @pl.when(is_self)
            def _():
                pltpu.make_async_copy(send.at[i, u], slots(u), rs.at[s]).start()

            @pl.when(jnp.logical_not(is_self))
            def _():
                pltpu.make_async_remote_copy(
                    src_ref=send.at[i, u], dst_ref=slots(u), send_sem=ss.at[i, u], recv_sem=rs.at[s],
                    device_id={"sp": chip, "tp": u}, device_id_type=MESH,
                ).start()

            return carry

        lax.fori_loop(0, 2 * heads, step, 0, unroll=True)

    def scatter_done(send, slots, ss, rs):
        def step(k, carry):
            i = k // 2
            u = lax.rem(k, 2)
            chip = t * heads + i
            is_self = jnp.logical_and(chip == s, u == t)

            @pl.when(jnp.logical_not(is_self))
            def _():
                pltpu.make_async_remote_copy(
                    src_ref=send.at[i, u], dst_ref=slots(u), send_sem=ss.at[i, u], recv_sem=rs.at[s],
                    device_id={"sp": chip, "tp": u}, device_id_type=MESH,
                ).wait_send()

            return carry

        lax.fori_loop(0, 2 * heads, step, 0)

    kv_slot = lambda u: kv_all.at[s, u]

    l_qs.wait()
    queries = dot(normed[...], vqs[...])
    for i in range(heads):
        cols = slice(i * hd, (i + 1) * hd)
        for u in range(2):
            top = queries[u * half : u * half + quarter, cols]
            low = queries[u * half + quarter : (u + 1) * half, cols]
            kv_send[i, u, half:] = jnp.concatenate([top, low], axis=1).astype(bf)
    scatter(kv_send, kv_slot, kv_ss, kv_rs)

    l_kw.wait()
    kvw[:, : kv_heads * hd] = dot(normed[...], vkw[...]).astype(bf)
    l_vw.wait()
    kvw[:, kv_heads * hd :] = dot(normed[...], vvw[...]).astype(bf)
    prev_copy = lambda to: pltpu.make_async_remote_copy(
        src_ref=kvw, dst_ref=kvw_prev, send_sem=p_ss, recv_sem=p_rs,
        device_id={"sp": to, "tp": t}, device_id_type=MESH,
    )

    l_qw.wait()
    qw = dot(normed[...], vqw[...])

    def forward(k, carry):
        src = k
        pltpu.make_async_remote_copy(
            src_ref=kv_send.at[0, 0], dst_ref=kv_all.at[src, t], send_sem=kv_ss.at[0, 0],
            recv_sem=kv_rs.at[src], device_id={"sp": s, "tp": other}, device_id_type=MESH,
        ).wait_recv()
        to_partner(kv_all.at[src, t, :half], kv_all.at[src, t, :half], f_ss.at[src], f_rs.at[src]).start()
        return carry

    def forward_arrived(k, carry):
        to_partner(kv_all.at[k, other, :half], kv_all.at[k, other, :half], f_ss.at[k], f_rs.at[k]).wait_recv()
        return carry

    def forward_sent(k, carry):
        to_partner(kv_all.at[k, t, :half], kv_all.at[k, t, :half], f_ss.at[k], f_rs.at[k]).wait_send()
        return carry

    def take_q(k, carry):
        slab = kv_all[k, t, half:].astype(f32)
        zero = jnp.zeros((quarter, hd), f32)
        both = jnp.concatenate(
            [
                jnp.concatenate([slab[:, :hd], zero], axis=1),
                jnp.concatenate([slab[:, hd:], zero], axis=1),
            ],
            axis=0,
        )
        q_pad[pl.ds(pl.multiple_of(k * half, half), half), :] = both.astype(bf)
        return carry

    b_copy.wait_recv()
    head_bias = bias_buf[s // heads, pl.ds(lax.rem(s, heads), 1), :][:, :1]

    kt = 2 * rows
    chunk = 4 * half
    later = (
        lax.broadcasted_iota(jnp.int32, (kt, kt), 0) > lax.broadcasted_iota(jnp.int32, (kt, kt), 1)
    ).astype(bf)
    row = lax.broadcasted_iota(jnp.int32, (chunk, kt), 0)
    lane = lax.broadcasted_iota(jnp.int32, (chunk, kt), 1)
    q_at = (row // half) * rows + t * half + lax.rem(row, half)
    scale = LOG2E * hd**-0.5

    def tile_of(n):
        return kv_all[2 * n : 2 * n + 2, :, :half].reshape(kt, 2 * hd)

    owner = s // heads
    slot = lax.rem(s, heads)
    n_chunks = n_sp // 4

    def arrive(qc):
        lax.fori_loop(qc * 4, qc * 4 + 4, forward, 0, unroll=True)
        lax.fori_loop(qc * 4, qc * 4 + 4, take_q, 0, unroll=True)

    arrive(0)
    for qc in range(n_chunks):
        if qc + 1 < n_chunks:
            arrive(qc + 1)
        if qc + 2 == n_chunks:
            @pl.when(s < n_sp - 1)
            def _():
                prev_copy(s + 1).start()

        lax.fori_loop(qc * 4, qc * 4 + 4, forward_arrived, 0, unroll=True)
        last = 2 * qc + 1
        carry = jnp.zeros((chunk, 1), f32)
        carries = {}
        for n in range(last, -1, -1):
            low = chunk // 2 if n == last else 0
            qs = q_pad[qc * chunk + low : (qc + 1) * chunk, :]
            z = dot_t(qs, tile_of(n)) * scale + head_bias
            pos = jnp.maximum(z, 0.0)
            neg = z - pos
            soft = jnp.log2(1.0 + jnp.exp2(neg - pos))
            drop = pos + soft
            hold = neg - soft
            if n >= last - 1:
                usable = (lane + (n - 2 * qc) * kt < q_at)[low:]
                drop = jnp.where(usable, drop, 0.0)
                hold = jnp.where(usable, hold, -jnp.inf)
            suffix = dot(drop.astype(bf), later)
            staged[low:, n * kt : (n + 1) * kt] = hold - suffix
            carries[n] = carry[low:]
            step = suffix[:, :1] + drop[:, :1]
            if low:
                step = jnp.concatenate([jnp.zeros((low, 1), f32), step], axis=0)
            carry = carry + step
        acc = None
        for n in range(last - 1, -1, -1):
            weights = jnp.exp2(staged[:, n * kt : (n + 1) * kt] - carries[n]).astype(bf)
            res = dot(weights, tile_of(n))
            acc = res if acc is None else acc + res
        low = chunk // 2
        weights = jnp.exp2(staged[low:, last * kt : (last + 1) * kt] - carries[last]).astype(bf)
        tail = dot(weights, tile_of(last))
        acc = jnp.concatenate([acc[:low], acc[low:] + tail], axis=0)
        for b in range(4):
            top = acc[b * half : b * half + quarter, hd:]
            bot = acc[b * half + quarter : (b + 1) * half, hd:]
            o_send[qc * 4 + b] = jnp.concatenate([top, bot], axis=1).astype(bf)

        def give(k, carry):
            is_self = jnp.logical_and(k == s, t == owner)

            @pl.when(is_self)
            def _():
                pltpu.make_async_copy(o_send.at[k], o_recv.at[slot, t], o_rs.at[slot, t]).start()

            @pl.when(jnp.logical_not(is_self))
            def _():
                pltpu.make_async_remote_copy(
                    src_ref=o_send.at[k], dst_ref=o_recv.at[slot, t], send_sem=o_ss.at[k],
                    recv_sem=o_rs.at[slot, t], device_id={"sp": k, "tp": owner}, device_id_type=MESH,
                ).start()

            return carry

        lax.fori_loop(qc * 4, qc * 4 + 4, give, 0)

    @pl.when(s == 0)
    def _():
        kvw_prev[...] = jnp.zeros_like(kvw_prev)

    @pl.when(s > 0)
    def _():
        prev_copy(s - 1).wait_recv()

    two = 2 * rows
    r_iota = lax.broadcasted_iota(jnp.int32, (two, two), 0)
    c_iota = lax.broadcasted_iota(jnp.int32, (two, two), 1)
    dist = lax.rem(r_iota, rows) + rows - c_iota
    in_window = (dist >= 0) & (dist < WINDOW) & ((c_iota >= rows) | (s > 0))
    first_rows = lax.broadcasted_iota(jnp.int32, (two, 1), 0) < rows
    for g in range(kv_heads):
        cols = slice(g * hd, (g + 1) * hd)
        v_cols = slice((kv_heads + g) * hd, (kv_heads + g + 1) * hd)
        kk = jnp.concatenate([kvw_prev[:, cols], kvw[:, cols]], axis=0)
        vv = jnp.concatenate([kvw_prev[:, v_cols], kvw[:, v_cols]], axis=0)
        base = g * GROUP * hd
        qq = jnp.concatenate(
            [qw[:, base : base + hd], qw[:, base + hd : base + 2 * hd]], axis=0
        ).astype(bf)
        logits = jnp.where(in_window, dot_t(qq, kk) * hd**-0.5, -jnp.inf)
        sink = jnp.where(first_rows, sinks[GROUP * g], sinks[GROUP * g + 1])
        top = jnp.maximum(jnp.max(logits, axis=1, keepdims=True), sink)
        grown = jnp.exp(logits - top)
        total = jnp.sum(grown, axis=1, keepdims=True) + jnp.exp(sink - top)
        weights = (grown / total).astype(bf)
        res = dot(weights, vv)
        w_out_buf[:, base : base + 2 * hd] = jnp.concatenate([res[:rows], res[rows:]], axis=1).astype(bf)

    wf = w_out_buf[...].astype(f32)
    sq_send[0] = jnp.broadcast_to(jnp.sum(wf * wf, axis=1, keepdims=True), (rows, 128))

    sq_w = to_partner(sq_send.at[0], sq_recv.at[0], sq_ss.at[0], sq_rs.at[0])
    sq_w.start()

    l_ow.wait()
    total_w[...] = dot((wf * wgain[...].reshape(1, sw)).astype(bf), vow[...])
    sq_w.wait_recv()
    sw_cols = 2.0 * sw
    inv_w = lax.rsqrt((sq_send[0] + sq_recv[0])[:, :1] / sw_cols + EPS)

    def take_o(k, carry):
        pltpu.make_async_remote_copy(
            src_ref=o_send.at[0], dst_ref=o_recv.at[k // 2, lax.rem(k, 2)], send_sem=o_ss.at[0],
            recv_sem=o_rs.at[k // 2, lax.rem(k, 2)], device_id={"sp": s, "tp": other}, device_id_type=MESH,
        ).wait_recv()
        return carry

    lax.fori_loop(0, 2 * heads, take_o, 0)
    for j in range(heads // 2):
        for u in range(2):
            one = o_recv[2 * j, u].astype(f32)
            two_ = o_recv[2 * j + 1, u].astype(f32)
            s_out_buf[u * half : u * half + quarter, 2 * j * hd : 2 * (j + 1) * hd] = jnp.concatenate(
                [one[:, :hd], two_[:, :hd]], axis=1
            )
            s_out_buf[u * half + quarter : (u + 1) * half, 2 * j * hd : 2 * (j + 1) * hd] = jnp.concatenate(
                [one[:, hd:], two_[:, hd:]], axis=1
            )
    sf = s_out_buf[...]
    sq_send[1] = jnp.broadcast_to(jnp.sum(sf * sf, axis=1, keepdims=True), (rows, 128))
    gained = (sf * sgain[...].reshape(1, sw)).astype(bf)
    sq_s = to_partner(sq_send.at[1], sq_recv.at[1], sq_ss.at[1], sq_rs.at[1])
    sq_s.start()
    l_os.wait()
    n_cut = c_send.shape[0]
    cut = feats // n_cut
    for n in range(n_cut):
        comb[:, n * cut : (n + 1) * cut] = dot(gained, vos[:, n * cut : (n + 1) * cut])
    sq_s.wait_recv()
    inv_s = lax.rsqrt((sq_send[1] + sq_recv[1])[:, :1] / sw_cols + EPS)
    copies = []
    theirs = pl.ds(pl.multiple_of(other * half, half), half)
    mine = pl.ds(pl.multiple_of(t * half, half), half)
    for n in range(n_cut):
        cols = slice(n * cut, (n + 1) * cut)
        comb[:, cols] = comb[:, cols] * inv_s + total_w[:, cols] * inv_w
        c_send[n] = comb[theirs, cols].astype(bf)
        copy = to_partner(c_send.at[n], c_recv.at[n], c_ss.at[n], c_rs.at[n])
        copy.start()
        copies.append(copy)
    square = jnp.zeros((half, 1), f32)
    for n in range(n_cut):
        cols = slice(n * cut, (n + 1) * cut)
        copies[n].wait_recv()
        summed = (comb[mine, cols] + c_recv[n].astype(f32)).astype(bf).astype(f32)
        total_w[:half, cols] = summed
        square = square + jnp.sum(summed * summed, axis=1, keepdims=True)
    inv = lax.rsqrt(square / feats + EPS)
    out[...] = (total_w[:half, :] * inv * post_gain[...].reshape(1, feats)).astype(bf)

    x_copy.wait_send()
    b_copy.wait_send()
    scatter_done(kv_send, kv_slot, kv_ss, kv_rs)
    lax.fori_loop(0, n_sp, forward_sent, 0)

    @pl.when(s < n_sp - 1)
    def _():
        prev_copy(s + 1).wait_send()

    def gave(k, carry):
        @pl.when(jnp.logical_not(jnp.logical_and(k == s, t == owner)))
        def _():
            pltpu.make_async_remote_copy(
                src_ref=o_send.at[k], dst_ref=o_recv.at[slot, t], send_sem=o_ss.at[k],
                recv_sem=o_rs.at[slot, t], device_id={"sp": k, "tp": owner}, device_id_type=MESH,
            ).wait_send()

        return carry

    lax.fori_loop(0, n_sp, gave, 0)
    sq_w.wait_send()
    sq_s.wait_send()
    for copy in copies:
        copy.wait_send()


def one_kernel(n_sp, *args):
    tokens, pre_gain, wqs, wks, wvs, wqw, wkw, wvw, bias, sinks, sgain, wgain, wos, wow, post_gain = args
    bf = jnp.bfloat16
    f32 = jnp.float32
    rows, feat_half = tokens.shape
    feats = 2 * feat_half
    half = rows // 2
    hd = HEAD_DIM
    heads = wqs.shape[1] // hd
    sw = wqs.shape[1]
    wide = 2 * hd
    kvw_cols = wkw.shape[1] + wvw.shape[1]
    assert 2 * heads == n_sp and rows == WINDOW
    v = pltpu.VMEM
    dma = pltpu.SemaphoreType.DMA
    anywhere = pl.BlockSpec(memory_space=pl.ANY)
    vmem = pl.BlockSpec(memory_space=pltpu.VMEM)
    n_cut = 4
    scratch = [
        v(pre_gain.shape, f32), pltpu.SMEM(bias.shape, f32), pltpu.SMEM(sinks.shape, f32),
        v(sgain.shape, f32), v(wgain.shape, f32), v(post_gain.shape, f32),
        v((2, rows, feat_half), bf), v((2, heads, 128), f32), v((rows, feats), bf),
        v(wqs.shape, bf), v(wks.shape, bf), v(wvs.shape, bf), v(wqw.shape, bf), v(wkw.shape, bf),
        v(wvw.shape, bf), v(wos.shape, bf), v(wow.shape, bf),
        v((heads, 2, half + half // 2, wide), bf), v((n_sp, 2, half + half // 2, wide), bf),
        v((n_sp * half, wide), bf), v((4 * half, n_sp * rows), f32),
        v((rows, kvw_cols), bf), v((rows, kvw_cols), bf), v((rows, sw), bf),
        v((n_sp, half // 2, wide), bf), v((heads, 2, half // 2, wide), bf), v((rows, sw), f32),
        v((2, rows, 128), f32), v((2, rows, 128), f32), v((rows, feats), f32), v((rows, feats), f32),
        v((n_cut, half, feats // n_cut), bf), v((n_cut, half, feats // n_cut), bf),
        dma((14,)), dma, dma, dma, dma, dma, dma((heads, 2)), dma((n_sp,)),
        dma((n_sp,)), dma((n_sp,)), dma, dma, dma((n_sp,)), dma((heads, 2)), dma((2,)), dma((2,)),
        dma((n_cut,)), dma((n_cut,)),
    ]
    return pl.pallas_call(
        functools.partial(kernel, n_sp),
        out_shape=jax.ShapeDtypeStruct((half, feats), bf),
        in_specs=[anywhere] * len(args),
        out_specs=vmem,
        scratch_shapes=scratch,
        compiler_params=pltpu.CompilerParams(
            collective_id=0, has_side_effects=True, vmem_limit_bytes=67043328
        ),
        name="layer",
    )(*args)


def passed_along(value, axis, steps):
    count = lax.axis_size(axis)
    initial, last = (max(0, -steps), min(count, count - steps))
    return lax.ppermute(value, axis, [(source, source + steps) for source in range(initial, last)])


def rounded(values):
    return lax.optimization_barrier(values.astype(jnp.bfloat16)).astype(jnp.float32)


def norm_rows(values, gain):
    stats = jnp.mean(values * values, axis=-1, keepdims=True)
    return values * lax.rsqrt(stats + EPS) * gain


def stick_block(queries, key_pair, head_bias, key_mask, carried):
    result, logsum = carried
    head_count = queries.shape[1]
    key_rows = key_pair[0].reshape(key_pair.shape[1], head_count, HEAD_DIM)
    values = key_pair[1].reshape(key_pair.shape[1], head_count, HEAD_DIM)
    scores = jnp.einsum(
        "thd,shd->hts", queries, key_rows, preferred_element_type=jnp.float32
    ) * HEAD_DIM ** (-0.5)
    scores = scores + head_bias[:, None, None]
    usable = key_mask[None]
    log_keep = jnp.where(usable, jax.nn.log_sigmoid(-scores), 0.0)
    suffix = lax.cumsum(log_keep, axis=2, reverse=True) - log_keep
    stick_weights = jnp.where(
        usable, jnp.exp(jax.nn.log_sigmoid(scores) + suffix + logsum[:, :, None]), 0.0
    )
    stick_weights = stick_weights.astype(jnp.bfloat16)
    result = result + jnp.einsum(
        "hts,shd->htd", stick_weights, values, preferred_element_type=jnp.float32
    )
    logsum = logsum + jnp.sum(log_keep, axis=2)
    return (result, logsum)


def by_collectives(
    tokens,
    pre_gain,
    w_query_stick,
    w_key_stick,
    w_value_stick,
    w_query_window,
    w_key_window,
    w_value_window,
    stick_bias,
    sinks,
    stick_gain,
    window_gain,
    w_out_stick,
    w_out_window,
    post_gain,
):
    gathered = lax.all_gather(tokens, "tp", axis=1, tiled=True)
    normed = norm_rows(gathered.astype(jnp.float32), pre_gain).astype(jnp.bfloat16)

    def project(weight):
        return jnp.dot(normed, weight, preferred_element_type=jnp.float32).astype(jnp.bfloat16)

    tok_rows = normed.shape[0]
    dev_index = lax.axis_index("sp")
    dev_count = lax.axis_size("sp")
    query_stick = project(w_query_stick)
    stick_heads = query_stick.shape[1] // HEAD_DIM
    queries = query_stick.reshape(tok_rows, stick_heads, HEAD_DIM)
    own_pair = jnp.stack([project(w_key_stick), project(w_value_stick)])
    pair_width = own_pair.shape[2]
    positions = jnp.arange(tok_rows, dtype=jnp.int32)
    initial = (
        jnp.zeros((stick_heads, tok_rows, HEAD_DIM), jnp.float32),
        jnp.zeros((stick_heads, tok_rows), jnp.float32),
    )
    collected = own_pair[None]
    for section_index in range(dev_count.bit_length() - 1):
        arrived = passed_along(collected, "sp", 2**section_index)
        collected = jnp.concatenate([arrived, collected], axis=0)
    per_group = min(dev_count, 8)
    group_count = dev_count // per_group
    grouped = collected.reshape(group_count, per_group, 2, tok_rows, pair_width)
    grouped = grouped.transpose(0, 2, 1, 3, 4).reshape(
        group_count, 2, per_group * tok_rows, pair_width
    )
    first_source = dev_index - (dev_count - 1)
    group_starts = (first_source + jnp.arange(group_count, dtype=jnp.int32) * per_group) * tok_rows
    query_pos = dev_index * tok_rows + positions
    span_offs = jnp.arange(per_group * tok_rows, dtype=jnp.int32)

    def visit_group(carried, inputs):
        key_pair, start_pos = inputs
        key_pos = start_pos + span_offs
        key_mask = (key_pos[None, :] >= 0) & (key_pos[None, :] < query_pos[:, None])
        return (stick_block(queries, key_pair, stick_bias, key_mask, carried), None)

    (stick_sum, _), _ = lax.scan(visit_group, initial, (grouped, group_starts), reverse=True)
    stick_out = (
        stick_sum.transpose(1, 0, 2).reshape(tok_rows, stick_heads * HEAD_DIM).astype(jnp.bfloat16)
    )
    query_window = project(w_query_window)
    window_pair = jnp.stack([project(w_key_window), project(w_value_window)])
    kv_heads = window_pair.shape[2] // HEAD_DIM
    previous = passed_along(window_pair, "sp", 1)
    extended = jnp.concatenate([previous, window_pair], axis=1)
    block_count = tok_rows // WINDOW
    extended = extended.reshape(2, block_count + 1, WINDOW, kv_heads, HEAD_DIM)
    banded = jnp.concatenate([extended[:, :-1], extended[:, 1:]], axis=2)
    q_blocks = query_window.reshape(block_count, WINDOW, kv_heads, GROUP, HEAD_DIM)
    logits = jnp.einsum(
        "nqhgd,nchd->nhgqc", q_blocks, banded[0], preferred_element_type=jnp.float32
    ) * HEAD_DIM ** (-0.5)
    query_offs = jnp.arange(WINDOW, dtype=jnp.int32)[:, None]
    key_offs = jnp.arange(2 * WINDOW, dtype=jnp.int32)[None, :]
    distance = query_offs + WINDOW - key_offs
    key_pos = (
        dev_index * tok_rows
        + jnp.arange(block_count, dtype=jnp.int32)[:, None] * WINDOW
        - WINDOW
        + key_offs
    )
    usable = ((distance >= 0) & (distance < WINDOW))[None] & (key_pos >= 0)[:, None, :]
    logits = jnp.where(usable[:, None, None], logits, -jnp.inf)
    sink_logit = sinks.reshape(kv_heads, GROUP)[None, :, :, None, None]
    row_top = jnp.maximum(jnp.max(logits, axis=-1, keepdims=True), sink_logit)
    weights_exp = jnp.exp(logits - row_top)
    normalizer = jnp.sum(weights_exp, axis=-1, keepdims=True) + jnp.exp(sink_logit - row_top)
    window_weights = (weights_exp / normalizer).astype(jnp.bfloat16)
    window_sum = jnp.einsum(
        "nhgqc,nchd->nqhgd", window_weights, banded[1], preferred_element_type=jnp.float32
    )
    window_out = window_sum.reshape(tok_rows, query_window.shape[1]).astype(jnp.bfloat16)
    stick_float = stick_out.astype(jnp.float32)
    window_float = window_out.astype(jnp.float32)
    squares = lax.psum(
        (jnp.sum(stick_float * stick_float, axis=1), jnp.sum(window_float * window_float, axis=1)),
        "tp",
    )
    stick_normed = (
        stick_float * lax.rsqrt(squares[0][:, None] / (stick_gain.shape[0] * lax.axis_size("tp")) + EPS) * stick_gain
    ).astype(jnp.bfloat16)
    window_normed = (
        window_float * lax.rsqrt(squares[1][:, None] / (window_gain.shape[0] * lax.axis_size("tp")) + EPS) * window_gain
    ).astype(jnp.bfloat16)
    total = jnp.dot(stick_normed, w_out_stick, preferred_element_type=jnp.float32)
    combined = lax.psum_scatter(
        (total + jnp.dot(window_normed, w_out_window, preferred_element_type=jnp.float32)).astype(
            jnp.bfloat16
        ),
        "tp",
        scatter_dimension=0,
        tiled=True,
    ).astype(jnp.float32)
    combined = rounded(combined)
    return norm_rows(combined, post_gain).astype(jnp.bfloat16)


def solution(mesh):
    in_specs = (
        P("sp", "tp"),
        P(),
        P(None, "tp"),
        P(None, "tp"),
        P(None, "tp"),
        P(None, "tp"),
        P(None, "tp"),
        P(None, "tp"),
        P("tp"),
        P("tp"),
        P("tp"),
        P("tp"),
        P("tp", None),
        P("tp", None),
        P(),
    )
    n_sp, n_tp = mesh.shape["sp"], mesh.shape["tp"]

    def shards(*args):
        heads = args[2].shape[1] // HEAD_DIM
        if n_tp == 2 and n_tp * heads == n_sp and args[0].shape[0] == WINDOW and n_sp % 4 == 0:
            return one_kernel(n_sp, *args)
        return by_collectives(*args)

    return jax.shard_map(
        shards,
        mesh=mesh,
        in_specs=in_specs,
        out_specs=P(("sp", "tp"), None),
        check_vma=False,
    )
```

profile of v0, /device:TPU:1, one launch (start us, length us, event | category | flops | bytes accessed | tf_op | source)
XLA Modules:
  0.0 448.4 jit_solution(1177120498074783569)
XLA Ops:
  6.5 20.1 %all_gather.3 = bf16[128,2048]{1,0:T(8,128)(2,1)S(1)} all-gather(bf16[128,256]{1,0:T(8,128)(2,1)} %param.17), channel_id=1, replica_groups=mesh['sp'=64,'tp'=8] {'tp'}, dimensions={1}, use_global_device_ids=true | all-gather | bytes 589824 | tf_op jit(solution)/shard_map/all_gather | solution.py:532
  26.9 1.4 fusion.22
  28.3 1.4 fusion.21
  29.7 1.3 collective-permute-start
  31.0 1.5 collective-permute-done
  32.6 1.8 collective-permute-start.1
  34.4 1.9 collective-permute-done.1
  36.3 14.4 %collective-permute-start.2 = (bf16[4,2,128,128]{3,2,1,0:T(8,128)(2,1)S(1)}, bf16[4,2,128,128]{3,2,1,0:T(8,128)(2,1)S(1)}, u32[]{:S(2)}, u32[]{:S(2)}) collective-permute-start(bf16[4,2,128,128]{3,2,1,0:T(8,128)(2,1)S(1)} %pad_maximum_fusion.1), channel_id=1, source_target_pairs={{0,32},{8,40},{16,48},{24,56},{32,64},{40,72},{48,80},{56,88},{64,... | collective-permute-start | bytes 786440 | tf_op jit(solution)/shard_map/ppermute | solution.py:480
  50.7 10.2 %collective-permute-done.2 = bf16[4,2,128,128]{3,2,1,0:T(8,128)(2,1)S(1)} collective-permute-done((bf16[4,2,128,128]{3,2,1,0:T(8,128)(2,1)S(1)}, bf16[4,2,128,128]{3,2,1,0:T(8,128)(2,1)S(1)}, u32[]{:S(2)}, u32[]{:S(2)}) %collective-permute-start.2) | collective-permute-done | bytes 262176 | tf_op jit(solution)/shard_map/ppermute | solution.py:480
  61.0 5.6 %collective-permute-start.3 = (bf16[8,2,128,128]{3,2,1,0:T(8,128)(2,1)S(1)}, bf16[8,2,128,128]{3,2,1,0:T(8,128)(2,1)S(1)}, u32[]{:S(2)}, u32[]{:S(2)}) collective-permute-start(bf16[8,2,128,128]{3,2,1,0:T(8,128)(2,1)S(1)} %pad_maximum_fusion), channel_id=1, source_target_pairs={{0,64},{8,72},{16,80},{24,88},{32,96},{40,104},{48,112},{56,120},{... | collective-permute-start | bytes 1572872 | tf_op jit(solution)/shard_map/ppermute | solution.py:480
  66.7 10.6 %collective-permute-done.3 = bf16[8,2,128,128]{3,2,1,0:T(8,128)(2,1)S(1)} collective-permute-done((bf16[8,2,128,128]{3,2,1,0:T(8,128)(2,1)S(1)}, bf16[8,2,128,128]{3,2,1,0:T(8,128)(2,1)S(1)}, u32[]{:S(2)}, u32[]{:S(2)}) %collective-permute-start.3) | collective-permute-done | bytes 524320 | tf_op jit(solution)/shard_map/ppermute | solution.py:480
  80.8 6.0 %collective-permute-start.4 = (bf16[16,2,128,128]{3,2,1,0:T(8,128)(2,1)}, bf16[16,2,128,128]{3,2,1,0:T(8,128)(2,1)S(1)}, u32[]{:S(2)}, u32[]{:S(2)}) collective-permute-start(bf16[16,2,128,128]{3,2,1,0:T(8,128)(2,1)} %constant_dynamic-update-slice_fusion), channel_id=1, source_target_pairs={{0,128},{8,136},{16,144},{24,152},{32,160},{40,168},{48,176},{56,1... | collective-permute-start | bytes 3145736 | tf_op jit(solution)/shard_map/ppermute | solution.py:480
  87.6 1.3 collective-permute-start.6
  88.9 1.4 convolution_convert_fusion.2
  90.3 1.4 convolution_convert_fusion.1
  91.8 17.3 %collective-permute-done.4 = bf16[16,2,128,128]{3,2,1,0:T(8,128)(2,1)S(1)} collective-permute-done((bf16[16,2,128,128]{3,2,1,0:T(8,128)(2,1)}, bf16[16,2,128,128]{3,2,1,0:T(8,128)(2,1)S(1)}, u32[]{:S(2)}, u32[]{:S(2)}) %collective-permute-start.4) | collective-permute-done | bytes 1048608 | tf_op jit(solution)/shard_map/ppermute | solution.py:480
  113.6 34.5 %collective-permute-start.5 = (bf16[32,2,128,128]{3,2,1,0:T(8,128)(2,1)}, bf16[32,2,128,128]{3,2,1,0:T(8,128)(2,1)}, u32[]{:S(2)}, u32[]{:S(2)}) collective-permute-start(bf16[32,2,128,128]{3,2,1,0:T(8,128)(2,1)} %constant_dynamic-update-slice_fusion.5), channel_id=1, source_target_pairs={{0,256},{8,264},{16,272},{24,280},{32,288},{40,296},{48,304},{56,3... | collective-permute-start | bytes 6291464 | tf_op jit(solution)/shard_map/ppermute | solution.py:480
  149.1 40.3 %collective-permute-done.5 = bf16[32,2,128,128]{3,2,1,0:T(8,128)(2,1)} collective-permute-done((bf16[32,2,128,128]{3,2,1,0:T(8,128)(2,1)}, bf16[32,2,128,128]{3,2,1,0:T(8,128)(2,1)}, u32[]{:S(2)}, u32[]{:S(2)}) %collective-permute-start.5) | collective-permute-done | bytes 2097184 | tf_op jit(solution)/shard_map/ppermute | solution.py:480
  189.4 3.2 constant_dynamic-update-slice_fusion.17
  197.1 6.7 %copy.19 = bf16[8,2,8,128,128]{3,2,4,1,0:T(8,128)(2,1)} copy(bf16[8,2,8,128,128]{4,3,1,2,0:T(8,128)(2,1)} %bitcast.4) | data formatting | bytes 8388608 | tf_op jit(solution)/shard_map/transpose | solution.py:558
  203.9 7.3 %reshape.302 = bf16[8,2,1024,128]{2,3,1,0:T(8,128)(2,1)} reshape(bf16[8,2,8,128,128]{3,2,4,1,0:T(8,128)(2,1)} %copy.19) | data formatting | bytes 8388608 | tf_op jit(solution)/shard_map/reshape | solution.py:558
  211.2 71.4 %while.17 = (s32[]{:T(128)}, f32[2,128,64]{1,2,0:T(8,128)S(1)}, f32[2,128]{1,0:T(2,128)S(1)}, s32[8]{0:T(128)S(1)}, bf16[8,2,1024,128]{2,3,1,0:T(8,128)(2,1)}, /...) while((s32[]{:T(128)}, f32[2,128,64]{1,2,0:T(8,128)S(1)}, ...), condition=%wide.region_5.6_spmd.clone, body=%wide.region_1.5_spmd.clone.sunk | while | flops 109366400 | bytes 13740244 | solution.py:572
  213.4 1.1 constant_dynamic-slice_fusion.3
  215.5 2.5 fusion.81
  218.4 1.5 fusion.83
  222.3 1.1 constant_dynamic-slice_fusion.3
  224.4 2.5 fusion.81
  227.3 1.5 fusion.83
  231.3 1.1 constant_dynamic-slice_fusion.3
  233.3 2.5 fusion.81
  236.2 1.5 fusion.83
  240.2 1.1 constant_dynamic-slice_fusion.3
  242.2 2.5 fusion.81
  245.2 1.5 fusion.83
  249.1 1.1 constant_dynamic-slice_fusion.3
  251.2 2.5 fusion.81
  254.1 1.5 fusion.83
  260.1 2.5 fusion.81
  263.0 1.5 fusion.83
  267.0 1.1 constant_dynamic-slice_fusion.3
  269.0 2.5 fusion.81
  271.9 1.5 fusion.83
  278.0 2.5 fusion.81
  280.9 1.5 fusion.83
  282.7 15.3 %all-reduce = (f32[128]{0:T(128)S(1)}, f32[128]{0:T(128)S(1)}) all-reduce(f32[128]{0:T(128)S(1)} %get-tuple-element.244, f32[128]{0:T(128)S(1)} %get-tuple-element.248), channel_id=1, replica_groups=mesh['sp'=64,'tp'=8] {'tp'}, use_global_device_ids=true, to_apply=%region_7.8 | all-reduce | flops 256 | bytes 2048 | tf_op jit(solution)/shard_map/psum | solution.py:610
  298.5 2.2 fusion.17
  300.7 138.4 %reduce-scatter.2.cloned.1.call-done = bf16[16,2048]{1,0:T(8,128)(2,1)} async-done(((bf16[128,2048]{1,0:T(8,128)(2,1)}), bf16[16,2048]{1,0:T(8,128)(2,1)}) %reduce-scatter.2.cloned.1.call-update) | async-done | bytes 65552 | tf_op jit(solution)/shard_map/reduce_scatter | solution.py:621
  440.0 1.6 fusion.31
  (176 shorter events, 47.9 us)
Async XLA Ops:
  6.5 291.5 %copy-start = (bf16[128,2048]{1,0:T(8,128)(2,1)S(1)}, bf16[128,2048]{1,0:T(8,128)(2,1)}, u32[]{:S(2)}) copy-start(bf16[128,2048]{1,0:T(8,128)(2,1)} %param.29) | copy-start | bytes 1572868
  6.5 80.2 %copy-start.7 = (f32[2048]{0:T(1024)S(1)}, f32[2048]{0:T(1024)}, u32[]{:S(2)}) copy-start(f32[2048]{0:T(1024)} %param.18) | copy-start | bytes 24580
  6.5 80.2 %copy-start.5 = (bf16[2048,64]{0,1:T(8,128)(2,1)S(1)}, bf16[2048,64]{0,1:T(8,128)(2,1)}, u32[]{:S(2)}) copy-start(bf16[2048,64]{0,1:T(8,128)(2,1)} %param.23) | copy-start | bytes 786436
  6.5 432.5 %reduce-scatter.2.cloned.1.call-start = ((), (), s32[]{:S(2)}) async-start(), calls=%async_computation.1 | async-start | bytes 589824 | tf_op jit(solution)/shard_map/reduce_scatter | solution.py:621
  26.7 60.5 %copy-start.6 = (bf16[2048,64]{0,1:T(8,128)(2,1)S(1)}, bf16[2048,64]{0,1:T(8,128)(2,1)}, u32[]{:S(2)}) copy-start(bf16[2048,64]{0,1:T(8,128)(2,1)} %param.24) | copy-start | bytes 786436
  29.7 2.8 collective-permute-start
  32.6 3.7 collective-permute-start.1
  36.3 24.6 %collective-permute-start.2 = (bf16[4,2,128,128]{3,2,1,0:T(8,128)(2,1)S(1)}, bf16[4,2,128,128]{3,2,1,0:T(8,128)(2,1)S(1)}, u32[]{:S(2)}, u32[]{:S(2)}) collective-permute-start(bf16[4,2,128,128]{3,2,1,0:T(8,128)(2,1)S(1)} %pad_maximum_fusion.1), channel_id=1, source_target_pairs={{0,32},{8,40},{16,48},{24,56},{32,64},{40,72},{48,80},{56,88},{64,... | collective-permute-start | bytes 786440 | tf_op jit(solution)/shard_map/ppermute | solution.py:480
  61.0 16.3 %collective-permute-start.3 = (bf16[8,2,128,128]{3,2,1,0:T(8,128)(2,1)S(1)}, bf16[8,2,128,128]{3,2,1,0:T(8,128)(2,1)S(1)}, u32[]{:S(2)}, u32[]{:S(2)}) collective-permute-start(bf16[8,2,128,128]{3,2,1,0:T(8,128)(2,1)S(1)} %pad_maximum_fusion), channel_id=1, source_target_pairs={{0,64},{8,72},{16,80},{24,88},{32,96},{40,104},{48,112},{56,120},{... | collective-permute-start | bytes 1572872 | tf_op jit(solution)/shard_map/ppermute | solution.py:480
  80.8 28.3 %collective-permute-start.4 = (bf16[16,2,128,128]{3,2,1,0:T(8,128)(2,1)}, bf16[16,2,128,128]{3,2,1,0:T(8,128)(2,1)S(1)}, u32[]{:S(2)}, u32[]{:S(2)}) collective-permute-start(bf16[16,2,128,128]{3,2,1,0:T(8,128)(2,1)} %constant_dynamic-update-slice_fusion), channel_id=1, source_target_pairs={{0,128},{8,136},{16,144},{24,152},{32,160},{40,168},{48,176},{56,1... | collective-permute-start | bytes 3145736 | tf_op jit(solution)/shard_map/ppermute | solution.py:480
  87.5 61.2 %copy-start.2 = (f32[2]{0:T(128)S(1)}, f32[2]{0:T(128)}, u32[]{:S(2)}) copy-start(f32[2]{0:T(128)} %param.26) | copy-start | bytes 28
  87.6 60.7 %collective-permute-start.6 = (bf16[2,128,64]{1,2,0:T(8,128)(2,1)S(1)}, bf16[2,128,64]{1,2,0:T(8,128)(2,1)S(1)}, u32[]{:S(2)}, u32[]{:S(2)}) collective-permute-start(bf16[2,128,64]{1,2,0:T(8,128)(2,1)S(1)} %pad_maximum_fusion.3), channel_id=1, source_target_pairs={{0,8},{8,16},{16,24},{24,32},{32,40},{40,48},{48,56},{56,64},{64,7... | collective-permute-start | bytes 98312 | tf_op jit(solution)/shard_map/ppermute | solution.py:480
  113.6 75.8 %collective-permute-start.5 = (bf16[32,2,128,128]{3,2,1,0:T(8,128)(2,1)}, bf16[32,2,128,128]{3,2,1,0:T(8,128)(2,1)}, u32[]{:S(2)}, u32[]{:S(2)}) collective-permute-start(bf16[32,2,128,128]{3,2,1,0:T(8,128)(2,1)} %constant_dynamic-update-slice_fusion.5), channel_id=1, source_target_pairs={{0,256},{8,264},{16,272},{24,280},{32,288},{40,296},{48,304},{56,3... | collective-permute-start | bytes 6291464 | tf_op jit(solution)/shard_map/ppermute | solution.py:480
  203.9 7.3 %copy-start.8 = (f32[2]{0:T(128)S(1)}, f32[2]{0:T(128)}, u32[]{:S(2)}) copy-start(f32[2]{0:T(128)} %param.25) | copy-start | bytes 28
  211.2 86.7 %copy-start.3 = (f32[128]{0:T(128)S(1)}, f32[128]{0:T(128)}, u32[]{:S(2)}) copy-start(f32[128]{0:T(128)} %param.27) | copy-start | bytes 1540
  211.2 87.2 %copy-start.4 = (f32[128]{0:T(128)S(1)}, f32[128]{0:T(128)}, u32[]{:S(2)}) copy-start(f32[128]{0:T(128)} %param.28) | copy-start | bytes 1540
  282.6 157.4 %copy-start.1 = (f32[2048]{0:T(1024)S(1)}, f32[2048]{0:T(1024)}, u32[]{:S(2)}) copy-start(f32[2048]{0:T(1024)} %param.31) | copy-start | bytes 24580
Sparse Core Ops, SparseCore 0:
  300.8 138.2 reduce-scatter.1
where the time goes:
time: 450 us; the launch traced here: 448 us
  waiting for transfers between devices  220 us (49%)
  starting transfers between devices  64.8 us (14%)
  other arithmetic  51.2 us (11%)
  local copies, waits for them, and re-layouts  43.1 us (10%)
  blocking collectives  35.4 us (8%)
  matrix products  19.1 us (4%)
  between operations  13.7 us (3%)
    reduce_scatter x1, waiting for transfers between devices, by_collectives(): lax.psum_scatter((total + jnp.dot(window_normed, w_out_window, preferred_...  138 us
    ppermute x7, waiting for transfers between devices, passed_along(): lax.ppermute(value, axis, [(source, source + steps) for source in range(i...  82 us
    ppermute x7, starting transfers between devices, passed_along(): lax.ppermute(value, axis, [(source, source + steps) for source in range(i...  64.8 us
    another operation x16, other arithmetic  20.6 us
    all_gather x1, blocking collectives, by_collectives(): gathered = lax.all_gather(tokens, 'tp', axis=1, tiled=True)  20.1 us
    psum x1, blocking collectives, by_collectives(): lax.psum((jnp.sum(stick_float * stick_float, axis=1), jnp.sum(window_floa...  15.3 us
    unnamed x34, local copies, waits for them, and re-layouts  13.8 us
    convert_element_type x8, other arithmetic, stick_block(): stick_weights = stick_weights.astype(jnp.bfloat16)  12 us
  transfers between devices with their start and end apart: 8, of which 7 were waited for; matrix products, arithmetic and copies ran while one was open for 2% of the time, Pallas kernels for 0%

commit v1 on v0

v1 whole, which is shorter than its diff:
```python
import functools

import jax
import jax.numpy as jnp
from jax import lax
from jax.experimental import pallas as pl
from jax.experimental.pallas import tpu as pltpu
from jax.sharding import PartitionSpec as P

HEAD_DIM = 64
WINDOW = 128
EPS = 1e-06
LOG2E = 1.4426950408889634
MESH = pl.DeviceIdType.MESH
NY = 8
NZ = 8
NT = 8
NX = 4
N_SP = NY * NZ


def dot(a, b):
    return jnp.dot(a, b, preferred_element_type=jnp.float32)


def dot_t(a, b):
    return lax.dot_general(a, b, (((1,), (1,)), ((), ())), preferred_element_type=jnp.float32)


def kernel(
    tokens, pre_gain_in, wqs, wks, wvs, wqw, wkw, wvw, bias_in, sinks_in, sgain_in, wgain_in, wos, wow,
    post_gain_in, out,
    pre_gain, bias, sinks, sgain, wgain, post_gain, x, sq_acc, normed, vqs, vkv, vqw, vkw, vvw, vos, vow,
    kv_all, q_all, o_seg, t_seg, kvw, kvw_prev, o_send, o_recv, t_send, t_recv,
    a_send, a_recv, b_send, b_recv, total,
    w_sem, tok_sem, x_ss, x_rs, kv_ss, kv_rs, q_ss, q_rs, p_ss, p_rs, o_ss, o_rs, t_ss, t_rs,
    a_ss, a_rs, b_ss, b_rs,
):
    bf = jnp.bfloat16
    f32 = jnp.float32
    s = lax.axis_index("sp")
    t = lax.axis_index("tp")
    z = s // NY
    y = lax.rem(s, NY)
    chip = t // 2
    core = lax.rem(t, 2)
    partner = chip * 2 + 1 - core
    rows, chunk = tokens.shape
    feats = NT * chunk
    hd = HEAD_DIM
    cut = rows // NT

    barrier = pltpu.get_barrier_semaphore()

    def greet(sp, tp):
        pl.semaphore_signal(barrier, inc=1, device_id={"sp": sp, "tp": tp}, device_id_type=MESH)

    for k in range(1, NZ):
        greet(lax.rem(z + k, NZ) * NY + y, t)
    for k in range(1, NY):
        greet(z * NY + lax.rem(y + k, NY), t)
    for k in range(1, NT):
        greet(s, lax.rem(t + k, NT))
    greet(lax.rem(s + 1, N_SP), t)
    greet(lax.rem(s + N_SP - 1, N_SP), t)

    half = rows // 2
    loads = [
        pltpu.make_async_copy(src, dst, w_sem.at[n])
        for n, (src, dst) in enumerate(
            [(wks, vkv.at[:, :rows]), (wvs, vkv.at[:, rows:]), (wqs, vqs), (wkw, vkw), (wvw, vvw), (wqw, vqw),
             (wow, vow), (wos.at[:half], vos.at[half:]), (wos.at[half:], vos.at[:half]),
             (bias_in, bias), (pre_gain_in, pre_gain), (sinks_in, sinks), (sgain_in, sgain),
             (wgain_in, wgain), (post_gain_in, post_gain)]
        )
    ]
    l_ks, l_vs, l_qs, l_kw, l_vw, l_qw, l_ow, l_os, l_os2, *l_small = loads
    tok_load = pltpu.make_async_copy(tokens, x.at[t], tok_sem)
    tok_load.start()
    for load in l_small + loads[:9]:
        load.start()

    for j in range(1, NZ):
        @pl.when(z + j >= NZ)
        def _():
            q_all[j] = jnp.zeros((rows, rows), bf)

        @pl.when(z - j < 0)
        def _():
            o_recv[j] = jnp.zeros((rows, rows), bf)
            t_recv[j] = jnp.zeros((8, rows), f32)

    for load in l_small:
        load.wait()
    tok_load.wait()
    pl.semaphore_wait(barrier, NZ + NY + NT - 3 + 2)

    def remote(src, dst, ss, rs, sp, tp):
        return pltpu.make_async_remote_copy(
            src_ref=src, dst_ref=dst, send_sem=ss, recv_sem=rs,
            device_id={"sp": sp, "tp": tp}, device_id_type=MESH,
        )

    sends = []

    def x_copy(slot, sem, tp):
        return remote(x.at[slot], x.at[slot], x_ss.at[sem], x_rs.at[slot], s, tp)

    def start(copy):
        copy.start()
        sends.append(copy)

    for dx in (2, 1, 3):
        start(x_copy(t, dx, lax.rem(chip + dx, NX) * 2 + core))
    start(x_copy(t, 0, partner))

    def squares(slot):
        v = x[slot].astype(f32)
        v = v * v
        return v[:, : chunk // 2] + v[:, chunk // 2 :]

    sq_acc[...] = squares(t)
    for dx in (1, 3, 2):
        slot = lax.rem(chip + NX - dx, NX) * 2 + core
        x_copy(slot, dx, partner).wait_recv()
        start(x_copy(slot, NX + dx, partner))
        sq_acc[...] += squares(slot)
    for dx in (0, 1, 3, 2):
        slot = lax.rem(chip + NX - dx, NX) * 2 + 1 - core
        x_copy(slot, dx, partner).wait_recv()
        sq_acc[...] += squares(slot)
    inv = lax.rsqrt(jnp.sum(sq_acc[...], axis=1, keepdims=True) * (1.0 / feats) + EPS)
    for k in range(NT):
        cols = slice(k * chunk, (k + 1) * chunk)
        normed[:, cols] = (x[k].astype(f32) * inv * pre_gain[cols].reshape(1, chunk)).astype(bf)

    lane = lax.broadcasted_iota(jnp.int32, (rows, rows), 1)
    left = lane < hd

    l_ks.wait()
    l_vs.wait()
    kv = dot(normed[...], vkv[...])
    keys = kv[:, :rows]
    values = pltpu.roll(kv[:, rows:], hd, 1)
    kv_all[y, 0] = jnp.where(left, keys, values).astype(bf)
    kv_all[y, 1] = jnp.where(left, values, keys).astype(bf)

    def kv_copy(slot, sem, to_y):
        return remote(kv_all.at[slot], kv_all.at[slot], kv_ss.at[sem], kv_rs.at[slot], z * NY + to_y, t)

    for k in (1, 7, 2, 6, 3, 5, 4):
        start(kv_copy(y, k, lax.rem(y + k, NY)))

    l_qs.wait()
    q_all[0] = dot(normed[...], vqs[...]).astype(bf)

    def q_copy(j, to_z):
        return remote(q_all.at[0], q_all.at[j], q_ss.at[j], q_rs.at[j], to_z * NY + y, t)

    for j in range(1, NZ):
        @pl.when(z - j >= 0)
        def _():
            q_copy(j, z - j).start()

    l_kw.wait()
    kvw[:, :hd] = dot(normed[...], vkw[...]).astype(bf)
    l_vw.wait()
    kvw[:, hd:] = dot(normed[...], vvw[...]).astype(bf)

    def prev_copy(to):
        return remote(kvw, kvw_prev, p_ss, p_rs, to, t)

    @pl.when(s < N_SP - 1)
    def _():
        prev_copy(s + 1).start()

    @pl.when(s == 0)
    def _():
        kvw_prev[...] = jnp.zeros_like(kvw_prev)

    l_qw.wait()
    qw = dot(normed[...], vqw[...])

    @pl.when(s > 0)
    def _():
        prev_copy(s - 1).wait_recv()

    two = 2 * rows
    r_iota = lax.broadcasted_iota(jnp.int32, (two, two), 0)
    c_iota = lax.broadcasted_iota(jnp.int32, (two, two), 1)
    dist = lax.rem(r_iota, rows) + rows - c_iota
    in_window = (dist >= 0) & (dist < WINDOW) & ((c_iota >= rows) | (s > 0))
    first_rows = lax.broadcasted_iota(jnp.int32, (two, 1), 0) < rows
    kk = jnp.concatenate([kvw_prev[...], kvw[...]], axis=0)
    qq = jnp.concatenate([jnp.where(left, qw, 0.0), jnp.where(left, pltpu.roll(qw, hd, 1), 0.0)], axis=0).astype(bf)
    logits = jnp.where(in_window, dot_t(qq, kk) * hd**-0.5, -jnp.inf)
    sink = jnp.where(first_rows, sinks[0], sinks[1])
    top = jnp.maximum(jnp.max(logits, axis=1, keepdims=True), sink)
    grown = jnp.exp(logits - top)
    norm = jnp.sum(grown, axis=1, keepdims=True) + jnp.exp(sink - top)
    res = dot((grown / norm).astype(bf), kk)
    w_out = jnp.where(left, pltpu.roll(res[:rows], hd, 1), res[rows:]).astype(bf).astype(f32)

    def give(send, recv, ss, rs, values, weights):
        sums = jnp.sum(values * values, axis=1, keepdims=True)
        high = sums.astype(bf)
        low = (sums - high.astype(f32)).astype(bf)
        send[:, :, feats:] = jnp.where(left, high.astype(f32), low.astype(f32)).astype(bf).reshape(NT, cut, rows)
        gained, w = weights
        n_cut = 4
        part = feats // n_cut
        for n in range(n_cut):
            cols = slice(n * part, (n + 1) * part)
            send[:, :, cols] = dot(gained, w[:, cols]).astype(bf).reshape(NT, cut, part)
        for dx, dc in ((2, 0), (2, 1), (1, 0), (1, 1), (3, 0), (3, 1), (0, 1)):
            to = lax.rem(chip + dx, NX) * 2 + lax.rem(core + dc, 2)
            start(remote(send.at[to], recv.at[t], ss.at[2 * dx + dc], rs.at[t], s, to))

    def take(send, recv, ss, rs, acc, width):
        own = send[t].astype(f32)
        acc[...] = own[:, :feats]
        sums = own[:, feats:]
        for dx, dc in ((0, 1), (1, 0), (1, 1), (3, 0), (3, 1), (2, 0), (2, 1)):
            frm = lax.rem(chip + dx, NX) * 2 + lax.rem(core + dc, 2)
            remote(send.at[frm], recv.at[frm], ss.at[2 * dx + dc], rs.at[frm], s, partner).wait_recv()
            got = recv[frm].astype(f32)
            acc[...] += got[:, :feats]
            sums += got[:, feats:]
        return lax.rsqrt((sums[:, :1] + sums[:, hd : hd + 1]) * (1.0 / width) + EPS)

    l_ow.wait()
    give(b_send, b_recv, b_ss, b_rs, w_out, ((w_out * wgain[...].reshape(1, rows)).astype(bf), vow))

    for j in range(1, NZ):
        @pl.when(z + j < NZ)
        def _():
            remote(
                q_all.at[0], q_all.at[j], q_ss.at[j], q_rs.at[j], lax.rem(z + j, NZ) * NY + y, t
            ).wait_recv()

    kt = 2 * rows
    mb = 2 * rows
    n_mb = NZ // 2
    later = (
        lax.broadcasted_iota(jnp.int32, (kt, kt), 0) > lax.broadcasted_iota(jnp.int32, (kt, kt), 1)
    ).astype(bf)
    row2 = lax.broadcasted_iota(jnp.int32, (mb, kt), 0)
    lane2 = lax.broadcasted_iota(jnp.int32, (mb, kt), 1)
    left2 = lax.broadcasted_iota(jnp.int32, (mb, rows), 1) < hd
    scale = LOG2E * hd**-0.5
    biases = (bias[0] * LOG2E, bias[1] * LOG2E)

    def step(i, carry):
        tile = lax.rem(y // 2 + i + i // 2 - 2 * (i // 3), NY // 2)
        for u in range(2):
            src = 2 * tile + u

            @pl.when(src != y)
            def _():
                kv_copy(src, 0, lax.rem(y + 1, NY)).wait_recv()

        pair = [kv_all[pl.ds(2 * tile, 2), h].reshape(kt, rows) for h in range(2)]
        for m in range(n_mb):
            part = slice(m * mb, (m + 1) * mb)
            queries = q_all[2 * m : 2 * m + 2].reshape(mb, rows).astype(f32)
            outs = []
            sums = []
            for h in range(2):
                qh = jnp.where(left2 if h == 0 else jnp.logical_not(left2), queries, 0.0).astype(bf)
                score = dot_t(qh, pair[h]) * scale + biases[h]
                pos = jnp.maximum(score, 0.0)
                neg = score - pos
                soft = jnp.log2(1.0 + jnp.exp2(neg - pos))
                drop = pos + soft
                hold = neg - soft
                if m == 0:
                    usable = (row2 >= rows) | (lane2 + tile * kt < row2 + y * rows)
                    drop = jnp.where(usable, drop, 0.0)
                    hold = jnp.where(usable, hold, -jnp.inf)
                suffix = dot(drop.astype(bf), later)
                weights = jnp.exp2(hold - suffix).astype(bf)
                outs.append(dot(weights, pair[h]))
                sums.append(suffix[:, :1] + drop[:, :1])
            o_seg[tile, part] = jnp.where(left2, outs[1], outs[0])
            t_seg[tile, part] = jnp.where(left2, sums[1], sums[0])
        return carry

    lax.fori_loop(0, NY // 2, step, 0)

    first = lax.broadcasted_iota(jnp.int32, (8, rows), 0) < 4
    own_t = None
    for j in range(NZ - 1, -1, -1):
        part = slice(j * rows, (j + 1) * rows)
        last = NY // 2 - 1
        acc = o_seg[last, part]
        carry = t_seg[last, part]
        for n in range(last - 1, -1, -1):
            acc = acc + jnp.exp2(-carry) * o_seg[n, part]
            carry = carry + t_seg[n, part]
        turned = carry.T
        compact = jnp.where(first, turned[0:8], turned[hd : hd + 8])
        if j == 0:
            own_t = compact
            own_o = acc
        else:
            o_send[j] = acc.astype(bf)
            t_send[j] = compact

            @pl.when(z + j < NZ)
            def _():
                to = (z + j) * NY + y
                remote(t_send.at[j], t_recv.at[j], t_ss.at[j], t_rs.at[j], to, t).start()
                remote(o_send.at[j], o_recv.at[j], o_ss.at[j], o_rs.at[j], to, t).start()

    for j in range(1, NZ):
        @pl.when(z - j >= 0)
        def _():
            frm = lax.rem(z + NZ - j, NZ) * NY + y
            remote(t_send.at[j], t_recv.at[j], t_ss.at[j], t_rs.at[j], frm, t).wait_recv()

    carry = own_t
    scales = []
    for j in range(1, NZ):
        scales.append(jnp.exp2(-carry))
        carry = carry + t_recv[j]
    scales = jnp.concatenate(scales + [jnp.zeros((rows - 8 * (NZ - 1), rows), f32)], axis=0).T
    acc = own_o
    for j in range(1, NZ):
        @pl.when(z - j >= 0)
        def _():
            frm = lax.rem(z + NZ - j, NZ) * NY + y
            remote(o_send.at[j], o_recv.at[j], o_ss.at[j], o_rs.at[j], frm, t).wait_recv()

    for j in range(1, NZ):
        at = 8 * (j - 1)
        acc = acc + jnp.where(left, scales[:, at : at + 1], scales[:, at + 4 : at + 5]) * o_recv[j].astype(f32)
    s_out = acc.astype(bf).astype(f32)
    gain = sgain[...].reshape(1, rows)
    gain = jnp.concatenate([gain[:, hd:], gain[:, :hd]], axis=1)
    l_os.wait()
    l_os2.wait()
    give(a_send, a_recv, a_ss, a_rs, s_out, ((s_out * gain).astype(bf), vos))

    inv_w = take(b_send, b_recv, b_ss, b_rs, total.at[1], NT * rows)
    total[1] = total[1] * inv_w
    inv_s = take(a_send, a_recv, a_ss, a_rs, total.at[0], NT * rows)
    both = (total[0] * inv_s + total[1]).astype(bf).astype(f32)
    stats = jnp.sum(both * both, axis=1, keepdims=True) * (1.0 / feats)
    out[...] = (both * lax.rsqrt(stats + EPS) * post_gain[...].reshape(1, feats)).astype(bf)

    for copy in sends:
        copy.wait_send()
    for j in range(1, NZ):
        @pl.when(z - j >= 0)
        def _():
            q_copy(j, z - j).wait_send()

        @pl.when(z + j < NZ)
        def _():
            to = (z + j) * NY + y
            remote(t_send.at[j], t_recv.at[j], t_ss.at[j], t_rs.at[j], to, t).wait_send()
            remote(o_send.at[j], o_recv.at[j], o_ss.at[j], o_rs.at[j], to, t).wait_send()

    @pl.when(s < N_SP - 1)
    def _():
        prev_copy(s + 1).wait_send()


def one_kernel(*args):
    tokens, pre_gain, wqs, wks, wvs, wqw, wkw, wvw, bias, sinks, sgain, wgain, wos, wow, post_gain = args
    bf = jnp.bfloat16
    f32 = jnp.float32
    rows, chunk = tokens.shape
    feats = NT * chunk
    cut = rows // NT
    v = pltpu.VMEM
    dma = pltpu.SemaphoreType.DMA
    anywhere = pl.BlockSpec(memory_space=pl.ANY)
    vmem = pl.BlockSpec(memory_space=pltpu.VMEM)
    scratch = [
        v(pre_gain.shape, f32), pltpu.SMEM(bias.shape, f32), pltpu.SMEM(sinks.shape, f32),
        v(sgain.shape, f32), v(wgain.shape, f32), v(post_gain.shape, f32),
        v((NT, rows, chunk), bf), v((rows, rows), f32), v((rows, feats), bf),
        v(wqs.shape, bf), v((feats, 2 * rows), bf), v(wqw.shape, bf), v(wkw.shape, bf), v(wvw.shape, bf),
        v(wos.shape, bf), v(wow.shape, bf),
        v((NY, 2, rows, rows), bf), v((NZ, rows, rows), bf),
        v((NY // 2, NZ * rows, rows), f32), v((NY // 2, NZ * rows, rows), f32),
        v((rows, rows), bf), v((rows, rows), bf),
        v((NZ, rows, rows), bf), v((NZ, rows, rows), bf), v((NZ, 8, rows), f32), v((NZ, 8, rows), f32),
        v((NT, cut, feats + rows), bf), v((NT, cut, feats + rows), bf),
        v((NT, cut, feats + rows), bf), v((NT, cut, feats + rows), bf), v((2, cut, feats), f32),
        dma((15,)), dma, dma((8,)), dma((NT,)), dma((NY,)), dma((NY,)), dma((NZ,)), dma((NZ,)), dma, dma,
        dma((NZ,)), dma((NZ,)), dma((NZ,)), dma((NZ,)), dma((NT,)), dma((NT,)), dma((NT,)), dma((NT,)),
    ]
    return pl.pallas_call(
        kernel,
        out_shape=jax.ShapeDtypeStruct((cut, feats), bf),
        in_specs=[anywhere] * len(args),
        out_specs=vmem,
        scratch_shapes=scratch,
        compiler_params=pltpu.CompilerParams(
            collective_id=0, has_side_effects=True, vmem_limit_bytes=67043328
        ),
        name="layer",
    )(*args)


def solution(mesh):
    in_specs = (
        P("sp", "tp"),
        P(),
        P(None, "tp"),
        P(None, "tp"),
        P(None, "tp"),
        P(None, "tp"),
        P(None, "tp"),
        P(None, "tp"),
        P("tp"),
        P("tp"),
        P("tp"),
        P("tp"),
        P("tp", None),
        P("tp", None),
        P(),
    )
    return jax.shard_map(
        one_kernel,
        mesh=mesh,
        in_specs=in_specs,
        out_specs=P(("sp", "tp"), None),
        check_vma=False,
    )
```

time: 450 us -> 61.9 us (0.14)
  the two profiles are of different devices: /device:TPU:1 before, /device:TPU:73 now
where the time goes in v1:
time: 61.9 us; the launch traced here: 61.7 us
  Pallas kernels  57.2 us (92%)
  local copies, waits for them, and re-layouts  4.48 us (7%)
    pallas_call x1, Pallas kernels, one_kernel(): pl.pallas_call(kernel, out_shape=jax.ShapeDtypeStruct((cut, feats), bf),...  57.2 us
    unnamed x5, local copies, waits for them, and re-layouts  4.48 us

profile of v1, /device:TPU:73, one launch (start us, length us, event | category | flops | bytes accessed | tf_op | source)
XLA Modules:
  0.0 61.7 jit_solution(15337978568997056968)
XLA Ops:
  0.0 0.0 copy-start
  0.0 2.0 %copy.16.wkw = bf16[2048,64]{1,0:T(8,128)(2,1)} copy(bf16[2048,64]{0,1:T(8,128)(2,1)} %param.21) | data formatting | bytes 524288 | tf_op args[6]
  2.0 0.0 copy-done
  2.0 1.0 %copy.17.wvw = bf16[2048,64]{1,0:T(8,128)(2,1)} copy(bf16[2048,64]{0,1:T(8,128)(2,1)S(1)} %copy-done) | data formatting | bytes 524288 | tf_op args[7]
  3.0 57.2 %layer.1 = bf16[16,2048]{1,0:T(8,128)(2,1)} custom-call(bf16[128,256]{1,0:T(8,128)(2,1)} %tokens.1, f32[2048]{0:T(1024)} %pre_gain_in.1, bf16[2048,128]{1,0:T(8,128)(2,1)} %wqs.1, bf16[2048,128]{1,0:T(8,128)(2,1)} %wks.1, bf16[2048,128]{1,0:T(8,128)(2,1)} %wvs.1, bf16[2048,128]{1,0:T(8,128)(2,1)} %wqw.1, bf16[2048,64]{1,0:T(8,128)(2,1)} %copy.16.wkw, ...), custom_call_target="tpu_custom_call" | custom-call | tf_op jit(solution)/shard_map/layer/pallas_call | solution.py:395
  60.2 1.5 %copy.19 = bf16[16,2048]{1,0:T(8,128)(2,1)} copy(bf16[16,2048]{1,0:T(8,128)(2,1)} %layer.1) | data formatting | bytes 131072
Async XLA Ops:
  0.0 2.0 %copy-start = (bf16[2048,64]{0,1:T(8,128)(2,1)S(1)}, bf16[2048,64]{0,1:T(8,128)(2,1)}, u32[]{:S(2)}) copy-start(bf16[2048,64]{0,1:T(8,128)(2,1)} %param.22) | copy-start | bytes 786436

commit v2 on v1

v2 whole, which is shorter than its diff:
```python
import functools

import jax
import jax.numpy as jnp
from jax import lax
from jax.experimental import pallas as pl
from jax.experimental.pallas import tpu as pltpu
from jax.sharding import PartitionSpec as P

HEAD_DIM = 64
WINDOW = 128
EPS = 1e-06
LOG2E = 1.4426950408889634
MESH = pl.DeviceIdType.MESH
NY = 8
NZ = 8
NT = 8
NX = 4
N_SP = NY * NZ


def dot(a, b):
    return jnp.dot(a, b, preferred_element_type=jnp.float32)


def dot_t(a, b):
    return lax.dot_general(a, b, (((1,), (1,)), ((), ())), preferred_element_type=jnp.float32)


def kernel(
    tokens, pre_gain_in, wqs, wks, wvs, wqw, wkw, wvw, bias_in, sinks_in, sgain_in, wgain_in, wos, wow,
    post_gain_in, out,
    pre_gain, bias, sinks, sgain, wgain, post_gain, x, sq_acc, normed, vqs, vkv, vqw, vkvw, vos, vow,
    kv_all, kv_other, q_all, q_other, o_seg, t_seg, kvw, qw_buf, kvw_prev, o_send, o_recv, t_send, t_recv,
    a_send, a_recv, b_send, b_recv, total,
    w_sem, tok_sem, x_ss, x_rs, kv_ss, kv_rs, q_ss, q_rs, p_ss, p_rs, o_ss, o_rs, t_ss, t_rs,
    a_ss, a_rs, b_ss, b_rs,
):
    bf = jnp.bfloat16
    f32 = jnp.float32
    s = lax.axis_index("sp")
    t = lax.axis_index("tp")
    z = s // NY
    y = lax.rem(s, NY)
    chip = t // 2
    core = lax.rem(t, 2)
    head = lax.rem(y, 2)
    y_other = y + 1 - 2 * head
    partner = chip * 2 + 1 - core
    rows, chunk = tokens.shape
    feats = NT * chunk
    hd = HEAD_DIM
    cut = rows // NT

    barrier = pltpu.get_barrier_semaphore()

    def greet(sp, tp):
        pl.semaphore_signal(barrier, inc=1, device_id={"sp": sp, "tp": tp}, device_id_type=MESH)

    for k in range(1, NZ):
        greet(lax.rem(z + k, NZ) * NY + y, t)
        greet(lax.rem(z + k, NZ) * NY + y_other, t)
    for k in range(1, NY):
        greet(z * NY + lax.rem(y + k, NY), t)
    for k in range(1, NT):
        greet(s, lax.rem(t + k, NT))
    greet(lax.rem(s + 1, N_SP), t)
    greet(lax.rem(s + N_SP - 1, N_SP), t)

    half = rows // 2
    loads = [
        pltpu.make_async_copy(src, dst, w_sem.at[n])
        for n, (src, dst) in enumerate(
            [(wks, vkv.at[:, :rows]), (wvs, vkv.at[:, rows:]), (wqs, vqs), (wkw, vkvw.at[:half]), (wvw, vkvw.at[half:]), (wqw, vqw),
             (wow, vow), (wos, vos),
             (bias_in, bias), (pre_gain_in, pre_gain), (sinks_in, sinks), (sgain_in, sgain),
             (wgain_in, wgain), (post_gain_in, post_gain)]
        )
    ]
    l_ks, l_vs, l_qs, l_kw, l_vw, l_qw, l_ow, l_os, *l_small = loads
    tok_load = pltpu.make_async_copy(tokens, x.at[t], tok_sem)
    tok_load.start()
    for load in l_small + loads[:8]:
        load.start()

    for j in range(1, NZ):
        @pl.when(z + j >= NZ)
        def _():
            q_all[j] = jnp.zeros((2, half, rows), bf)

        @pl.when(z - j < 0)
        def _():
            o_recv[j] = jnp.zeros((2, half, rows), bf)
            t_recv[j] = jnp.zeros((2, 8, rows), f32)

    for load in l_small:
        load.wait()
    tok_load.wait()
    pl.semaphore_wait(barrier, 2 * NZ + NY + NT - 4 + 2)

    def remote(src, dst, ss, rs, sp, tp):
        return pltpu.make_async_remote_copy(
            src_ref=src, dst_ref=dst, send_sem=ss, recv_sem=rs,
            device_id={"sp": sp, "tp": tp}, device_id_type=MESH,
        )

    sends = []

    def x_copy(slot, sem, tp):
        return remote(x.at[slot], x.at[slot], x_ss.at[sem], x_rs.at[slot], s, tp)

    def start(copy):
        copy.start()
        sends.append(copy)

    for dx in (2, 1, 3):
        start(x_copy(t, dx, lax.rem(chip + dx, NX) * 2 + core))
    start(x_copy(t, 0, partner))

    def squares(slot):
        v = x[slot].astype(f32)
        v = v * v
        return v[:, : chunk // 2] + v[:, chunk // 2 :]

    sq_acc[...] = squares(t)
    for dx in (1, 3, 2):
        slot = lax.rem(chip + NX - dx, NX) * 2 + core
        x_copy(slot, dx, partner).wait_recv()
        start(x_copy(slot, NX + dx, partner))
        sq_acc[...] += squares(slot)
    for dx in (0, 1, 3, 2):
        slot = lax.rem(chip + NX - dx, NX) * 2 + 1 - core
        x_copy(slot, dx, partner).wait_recv()
        sq_acc[...] += squares(slot)
    inv = lax.rsqrt(jnp.sum(sq_acc[...], axis=1, keepdims=True) * (1.0 / feats) + EPS)
    for k in range(NT):
        cols = slice(k * chunk, (k + 1) * chunk)
        normed[:, cols] = (x[k].astype(f32) * inv * pre_gain[cols].reshape(1, chunk)).astype(bf)

    left = lax.broadcasted_iota(jnp.int32, (rows, rows), 1) < hd
    left_half = left[:half]

    l_ks.wait()
    l_vs.wait()
    kv = dot(normed[...], vkv[...])
    keys, values = kv[:, :rows], kv[:, rows:]
    head0 = jnp.where(left, keys, pltpu.roll(values, hd, 1))
    head1 = jnp.where(left, pltpu.roll(keys, hd, 1), values)
    kv_all[y] = jnp.where(head == 0, head0, head1).astype(bf)
    kv_other[...] = jnp.where(head == 0, head1, head0).astype(bf)

    def kv_copy(src, slot, sem, to_y):
        return remote(src, kv_all.at[slot], kv_ss.at[sem], kv_rs.at[slot], z * NY + to_y, t)

    def kv_send(k):
        start(kv_copy(kv_other if k % 2 else kv_all.at[y], y, k, lax.rem(y + k, NY)))

    for k in (1, 7, 2, 6):
        kv_send(k)

    l_qs.wait()
    qs = dot(normed[...], vqs[...])
    q0 = jnp.where(left_half, qs[:half], pltpu.roll(qs[half:], hd, 1))
    q1 = jnp.where(left_half, pltpu.roll(qs[:half], hd, 1), qs[half:])
    q_all[0, 0] = jnp.where(head == 0, q0, q1).astype(bf)
    q_other[...] = jnp.where(head == 0, q1, q0).astype(bf)

    def q_copy(j, e, to_z):
        src = q_other if e else q_all.at[0, 0]
        return remote(
            src, q_all.at[j, e], q_ss.at[j, e], q_rs.at[j, e], to_z * NY + (y_other if e else y), t
        )

    start(q_copy(0, 1, z))
    for j in range(1, NZ):
        @pl.when(z - j >= 0)
        def _():
            q_copy(j, 0, z - j).start()
            q_copy(j, 1, z - j).start()

    l_kw.wait()
    l_vw.wait()
    kvw[...] = dot_t(normed[...], vkvw[...]).astype(bf)

    def prev_copy(to):
        return remote(kvw, kvw_prev, p_ss, p_rs, to, t)

    @pl.when(s < N_SP - 1)
    def _():
        prev_copy(s + 1).start()

    for k in (3, 5, 4):
        kv_send(k)

    @pl.when(s == 0)
    def _():
        kvw_prev[...] = jnp.zeros_like(kvw_prev)

    l_qw.wait()
    qw_buf[...] = dot(normed[...], vqw[...])

    def given(send, recv, ss, rs):
        for dx, dc in ((2, 0), (2, 1), (1, 0), (1, 1), (3, 0), (3, 1), (0, 1)):
            to = lax.rem(chip + dx, NX) * 2 + lax.rem(core + dc, 2)
            yield remote(send.at[to], recv.at[t], ss.at[2 * dx + dc], rs.at[t], s, to)

    def give(send, recv, ss, rs, values, weights):
        sums = jnp.sum(values * values, axis=1, keepdims=True)
        high = sums.astype(bf)
        low = (sums - high.astype(f32)).astype(bf)
        send[:, :, feats:] = jnp.where(left, high.astype(f32), low.astype(f32)).astype(bf).reshape(NT, cut, rows)
        gained, w = weights
        n_cut = 4
        part = feats // n_cut
        for n in range(n_cut):
            cols = slice(n * part, (n + 1) * part)
            send[:, :, cols] = dot(gained, w[:, cols]).astype(bf).reshape(NT, cut, part)
        for copy in given(send, recv, ss, rs):
            copy.start()

    def take(send, recv, ss, rs, acc, width):
        own = send[t].astype(f32)
        acc[...] = own[:, :feats]
        sums = own[:, feats:]
        for dx, dc in ((0, 1), (1, 0), (1, 1), (3, 0), (3, 1), (2, 0), (2, 1)):
            frm = lax.rem(chip + dx, NX) * 2 + lax.rem(core + dc, 2)
            remote(send.at[frm], recv.at[frm], ss.at[2 * dx + dc], rs.at[frm], s, partner).wait_recv()
            got = recv[frm].astype(f32)
            acc[...] += got[:, :feats]
            sums += got[:, feats:]
        return lax.rsqrt((sums[:, :1] + sums[:, hd : hd + 1]) * (1.0 / width) + EPS)

    def windowed():
        @pl.when(s > 0)
        def _():
            prev_copy(s - 1).wait_recv()

        two = 2 * rows
        r_iota = lax.broadcasted_iota(jnp.int32, (two, two), 0)
        c_iota = lax.broadcasted_iota(jnp.int32, (two, two), 1)
        dist = lax.rem(r_iota, rows) + rows - c_iota
        in_window = (dist >= 0) & (dist < WINDOW) & ((c_iota >= rows) | (s > 0))
        first_rows = lax.broadcasted_iota(jnp.int32, (two, 1), 0) < rows
        qw = qw_buf[...]
        kk = jnp.concatenate([kvw_prev[...], kvw[...]], axis=0)
        qq = jnp.concatenate([jnp.where(left, qw, 0.0), jnp.where(left, pltpu.roll(qw, hd, 1), 0.0)], axis=0).astype(bf)
        logits = jnp.where(in_window, dot_t(qq, kk) * hd**-0.5, -jnp.inf)
        sink = jnp.where(first_rows, sinks[0], sinks[1])
        top = jnp.maximum(jnp.max(logits, axis=1, keepdims=True), sink)
        grown = jnp.exp(logits - top)
        norm = jnp.sum(grown, axis=1, keepdims=True) + jnp.exp(sink - top)
        res = dot((grown / norm).astype(bf), kk)
        w_out = jnp.where(left, pltpu.roll(res[:rows], hd, 1), res[rows:]).astype(bf).astype(f32)

        l_ow.wait()
        give(b_send, b_recv, b_ss, b_rs, w_out, ((w_out * wgain[...].reshape(1, rows)).astype(bf), vow))

    def q_wait(j, e):
        frm = lax.rem(z + j, NZ) * NY + (y_other if e else y)
        remote(q_other, q_all.at[j, e], q_ss.at[j, e], q_rs.at[j, e], frm, t).wait_recv()

    q_wait(0, 1)
    for j in range(1, NZ):
        @pl.when(z + j < NZ)
        def _():
            q_wait(j, 0)
            q_wait(j, 1)

    kt = 2 * rows
    mb = 2 * rows
    n_mb = NZ * rows // mb
    later = (
        lax.broadcasted_iota(jnp.int32, (kt, kt), 0) > lax.broadcasted_iota(jnp.int32, (kt, kt), 1)
    ).astype(bf)
    row2 = lax.broadcasted_iota(jnp.int32, (mb, kt), 0)
    lane2 = lax.broadcasted_iota(jnp.int32, (mb, kt), 1)
    place = lax.rem(row2, half) + jnp.where(row2 < half, y, y_other) * rows
    left2 = lax.broadcasted_iota(jnp.int32, (mb, rows), 1) < hd
    scale = LOG2E * hd**-0.5
    head_bias = bias[head] * LOG2E

    def step(i, carry):
        @pl.when(i == 1)
        def _():
            windowed()

        tile = lax.rem(y // 2 + i + i // 2 - 2 * (i // 3), NY // 2)
        for u in range(2):
            src = 2 * tile + u

            @pl.when(src != y)
            def _():
                kv_copy(kv_other, src, 0, lax.rem(y + 1, NY)).wait_recv()

        straight = kv_all[pl.ds(2 * tile, 2)].reshape(kt, rows)
        turned = pltpu.roll(straight.astype(f32), hd, 1).astype(bf)
        for m in range(n_mb):
            part = slice(m * mb, (m + 1) * mb)
            per = mb // rows
            queries = q_all[m * per : (m + 1) * per].reshape(mb, rows).astype(f32)
            outs = []
            sums = []
            for u in range(2):
                qh = jnp.where(jnp.logical_not(left2) if u else left2, queries, 0.0).astype(bf)
                score = dot_t(qh, turned if u else straight) * scale + head_bias
                pos = jnp.maximum(score, 0.0)
                neg = score - pos
                soft = jnp.log2(1.0 + jnp.exp2(neg - pos))
                drop = pos + soft
                hold = neg - soft
                if m == 0:
                    usable = (row2 >= rows) | (lane2 + tile * kt < place + u * half)
                    drop = jnp.where(usable, drop, 0.0)
                    hold = jnp.where(usable, hold, -jnp.inf)
                suffix = dot(drop.astype(bf), later)
                weights = jnp.exp2(hold - suffix).astype(bf)
                outs.append(dot(weights, straight if u else turned))
                sums.append(suffix[:, :1] + drop[:, :1])
            o_seg[tile, part] = jnp.where(left2, outs[0], outs[1])
            t_seg[tile, part] = jnp.where(left2, sums[0], sums[1])
        return carry

    lax.fori_loop(0, NY // 2, step, 0)

    def to_owner(j, e, sp, which):
        if which:
            return remote(o_send.at[j, e], o_recv.at[j, e], o_ss.at[j, e], o_rs.at[j, e], sp, t)
        return remote(t_send.at[j], t_recv.at[j, e], t_ss.at[j, e], t_rs.at[j, e], sp, t)

    first = lax.broadcasted_iota(jnp.int32, (8, rows), 0) < 4
    for j in range(NZ - 1, -1, -1):
        part = slice(j * rows, (j + 1) * rows)
        last = NY // 2 - 1
        acc = o_seg[last, part]
        carry = t_seg[last, part]
        for n in range(last - 1, -1, -1):
            acc = acc + jnp.exp2(-carry) * o_seg[n, part]
            carry = carry + t_seg[n, part]
        over = carry.T
        compact = jnp.where(first, over[0:8], over[hd : hd + 8])
        o_send[j] = acc.astype(bf).reshape(2, half, rows)
        t_send[j] = compact
        if j == 0:
            own_t = compact
            own_o = acc[:half]
            for which in range(2):
                start(to_owner(0, 1, z * NY + y_other, which))
        else:
            @pl.when(z + j < NZ)
            def _():
                for e in range(2):
                    for which in range(2):
                        to_owner(j, e, (z + j) * NY + (y_other if e else y), which).start()

    def from_owner(j, e, which):
        frm = lax.rem(z + NZ - j, NZ) * NY + (y_other if e else y)
        to_owner(j, e, frm, which).wait_recv()

    def arrivals(which):
        from_owner(0, 1, which)
        for j in range(1, NZ):
            @pl.when(z - j >= 0)
            def _():
                from_owner(j, 0, which)
                from_owner(j, 1, which)

    arrivals(0)
    left8 = left[:8]
    carry = jnp.where(left8, own_t, t_recv[0, 1])
    scales = []
    for j in range(1, NZ):
        scales.append(jnp.exp2(-carry))
        carry = carry + jnp.where(left8, t_recv[j, 0], t_recv[j, 1])
    scales = jnp.concatenate(scales + [jnp.zeros((rows - 8 * (NZ - 1), rows), f32)], axis=0).T
    arrivals(1)
    acc = jnp.concatenate([own_o, o_recv[0, 1].astype(f32)], axis=0)
    for j in range(1, NZ):
        at = 8 * (j - 1)
        here = o_recv[j].reshape(rows, rows).astype(f32)
        acc = acc + jnp.where(left, scales[:, at : at + 1], scales[:, at + 4 : at + 5]) * here
    head0 = jnp.where(head == 0, acc[:half], acc[half:])
    head1 = jnp.where(head == 0, acc[half:], acc[:half])
    s_out = jnp.concatenate(
        [
            jnp.where(left_half, head0, pltpu.roll(head1, hd, 1)),
            jnp.where(left_half, pltpu.roll(head0, hd, 1), head1),
        ],
        axis=0,
    ).astype(bf).astype(f32)
    l_os.wait()
    give(a_send, a_recv, a_ss, a_rs, s_out, ((s_out * sgain[...].reshape(1, rows)).astype(bf), vos))

    inv_w = take(b_send, b_recv, b_ss, b_rs, total.at[1], NT * rows)
    total[1] = total[1] * inv_w
    inv_s = take(a_send, a_recv, a_ss, a_rs, total.at[0], NT * rows)
    both = (total[0] * inv_s + total[1]).astype(bf).astype(f32)
    stats = jnp.sum(both * both, axis=1, keepdims=True) * (1.0 / feats)
    out[...] = (both * lax.rsqrt(stats + EPS) * post_gain[...].reshape(1, feats)).astype(bf)

    for refs in ((a_send, a_recv, a_ss, a_rs), (b_send, b_recv, b_ss, b_rs)):
        for copy in given(*refs):
            copy.wait_send()
    for copy in sends:
        copy.wait_send()
    for j in range(1, NZ):
        for e in range(2):
            @pl.when(z - j >= 0)
            def _():
                q_copy(j, e, z - j).wait_send()

            @pl.when(z + j < NZ)
            def _():
                for which in range(2):
                    to_owner(j, e, (z + j) * NY + (y_other if e else y), which).wait_send()

    @pl.when(s < N_SP - 1)
    def _():
        prev_copy(s + 1).wait_send()


def one_kernel(*args):
    tokens, pre_gain, wqs, wks, wvs, wqw, wkw, wvw, bias, sinks, sgain, wgain, wos, wow, post_gain = args
    bf = jnp.bfloat16
    f32 = jnp.float32
    rows, chunk = tokens.shape
    feats = NT * chunk
    cut = rows // NT
    v = pltpu.VMEM
    dma = pltpu.SemaphoreType.DMA
    anywhere = pl.BlockSpec(memory_space=pl.ANY)
    vmem = pl.BlockSpec(memory_space=pltpu.VMEM)
    scratch = [
        v(pre_gain.shape, f32), pltpu.SMEM(bias.shape, f32), pltpu.SMEM(sinks.shape, f32),
        v(sgain.shape, f32), v(wgain.shape, f32), v(post_gain.shape, f32),
        v((NT, rows, chunk), bf), v((rows, rows), f32), v((rows, feats), bf),
        v(wqs.shape, bf), v((feats, 2 * rows), bf), v(wqw.shape, bf), v((rows, feats), bf),
        v(wos.shape, bf), v(wow.shape, bf),
        v((NY, rows, rows), bf), v((rows, rows), bf), v((NZ, 2, rows // 2, rows), bf), v((rows // 2, rows), bf),
        v((NY // 2, NZ * rows, rows), f32), v((NY // 2, NZ * rows, rows), f32),
        v((rows, rows), bf), v((rows, rows), f32), v((rows, rows), bf),
        v((NZ, 2, rows // 2, rows), bf), v((NZ, 2, rows // 2, rows), bf),
        v((NZ, 8, rows), f32), v((NZ, 2, 8, rows), f32),
        v((NT, cut, feats + rows), bf), v((NT, cut, feats + rows), bf),
        v((NT, cut, feats + rows), bf), v((NT, cut, feats + rows), bf), v((2, cut, feats), f32),
        dma((14,)), dma, dma((8,)), dma((NT,)), dma((NY,)), dma((NY,)), dma((NZ, 2)), dma((NZ, 2)), dma, dma,
        dma((NZ, 2)), dma((NZ, 2)), dma((NZ, 2)), dma((NZ, 2)), dma((NT,)), dma((NT,)), dma((NT,)), dma((NT,)),
    ]
    return pl.pallas_call(
        kernel,
        out_shape=jax.ShapeDtypeStruct((cut, feats), bf),
        in_specs=[anywhere] * len(args),
        out_specs=vmem,
        scratch_shapes=scratch,
        compiler_params=pltpu.CompilerParams(
            collective_id=0, has_side_effects=True, vmem_limit_bytes=67043328
        ),
        name="layer",
    )(*args[:6], wkw.T, wvw.T, *args[8:])


def solution(mesh):
    in_specs = (
        P("sp", "tp"),
        P(),
        P(None, "tp"),
        P(None, "tp"),
        P(None, "tp"),
        P(None, "tp"),
        P(None, "tp"),
        P(None, "tp"),
        P("tp"),
        P("tp"),
        P("tp"),
        P("tp"),
        P("tp", None),
        P("tp", None),
        P(),
    )
    return jax.shard_map(
        one_kernel,
        mesh=mesh,
        in_specs=in_specs,
        out_specs=P(("sp", "tp"), None),
        check_vma=False,
    )
```

time: 61.9 us -> 58.6 us (0.947)
  the two profiles are of different devices: /device:TPU:73 before, /device:TPU:1 now
where the time goes in v2:
time: 58.6 us; the launch traced here: 58 us
  Pallas kernels  56.5 us (96%)
  local copies, waits for them, and re-layouts  1.47 us (3%)
    pallas_call x1, Pallas kernels, one_kernel(): pl.pallas_call(kernel, out_shape=jax.ShapeDtypeStruct((cut, feats), bf),...  56.5 us
    unnamed x1, local copies, waits for them, and re-layouts  1.47 us

profile of v2, /device:TPU:1, one launch (start us, length us, event | category | flops | bytes accessed | tf_op | source)
XLA Modules:
  0.0 58.0 jit_solution(12213081243628175429)
XLA Ops:
  0.0 56.5 %layer.1 = bf16[16,2048]{1,0:T(8,128)(2,1)} custom-call(bf16[128,256]{1,0:T(8,128)(2,1)} %tokens.1, f32[2048]{0:T(1024)} %pre_gain_in.1, bf16[2048,128]{1,0:T(8,128)(2,1)} %wqs.1, bf16[2048,128]{1,0:T(8,128)(2,1)} %wks.1, bf16[2048,128]{1,0:T(8,128)(2,1)} %wvs.1, bf16[2048,128]{1,0:T(8,128)(2,1)} %wqw.1, bf16[64,2048]{1,0:T(8,128)(2,1)} %bitcast.2, ...), custom_call_target="tpu_custom_call" | custom-call | tf_op jit(solution)/shard_map/layer/pallas_call | solution.py:448
  56.5 1.5 %copy.17 = bf16[16,2048]{1,0:T(8,128)(2,1)} copy(bf16[16,2048]{1,0:T(8,128)(2,1)} %layer.1) | data formatting | bytes 131072

commit v3 on v2

--- a/solution.py
+++ b/solution.py
@@ -172,7 +172,7 @@
         )
 
     start(q_copy(0, 1, z))
-    for j in range(1, NZ):
+    for j in (1, 2, 3, 4, 5, 6, 7):
         @pl.when(z - j >= 0)
         def _():
             q_copy(j, 0, z - j).start()
@@ -259,16 +259,17 @@
         frm = lax.rem(z + j, NZ) * NY + (y_other if e else y)
         remote(q_other, q_all.at[j, e], q_ss.at[j, e], q_rs.at[j, e], frm, t).wait_recv()
 
-    q_wait(0, 1)
-    for j in range(1, NZ):
-        @pl.when(z + j < NZ)
-        def _():
-            q_wait(j, 0)
-            q_wait(j, 1)
+    def q_waits(js):
+        for j in js:
+            @pl.when(z + j < NZ)
+            def _():
+                if j:
+                    q_wait(j, 0)
+                q_wait(j, 1)
 
     kt = 2 * rows
     mb = 2 * rows
-    n_mb = NZ * rows // mb
+    per = mb // rows
     later = (
         lax.broadcasted_iota(jnp.int32, (kt, kt), 0) > lax.broadcasted_iota(jnp.int32, (kt, kt), 1)
     ).astype(bf)
@@ -279,6 +280,34 @@
     scale = LOG2E * hd**-0.5
     head_bias = bias[head] * LOG2E
 
+    def segment(m, tile, straight, turned):
+        part = slice(m * mb, (m + 1) * mb)
+        queries = q_all[m * per : (m + 1) * per].reshape(mb, rows).astype(f32)
+        outs = []
+        sums = []
+        for u in range(2):
+            qh = jnp.where(jnp.logical_not(left2) if u else left2, queries, 0.0).astype(bf)
+            score = dot_t(qh, turned if u else straight) * scale + head_bias
+            pos = jnp.maximum(score, 0.0)
+            neg = score - pos
+            soft = jnp.log2(1.0 + jnp.exp2(neg - pos))
+            drop = pos + soft
+            hold = neg - soft
+            if m == 0:
+                usable = (row2 >= rows) | (lane2 + tile * kt < place + u * half)
+                drop = jnp.where(usable, drop, 0.0)
+                hold = jnp.where(usable, hold, -jnp.inf)
+            suffix = dot(drop.astype(bf), later)
+            weights = jnp.exp2(hold - suffix).astype(bf)
+            outs.append(dot(weights, straight if u else turned))
+            sums.append(suffix[:, :1] + drop[:, :1])
+        o_seg[tile, part] = jnp.where(left2, outs[0], outs[1])
+        t_seg[tile, part] = jnp.where(left2, sums[0], sums[1])
+
+    def keys_of(tile):
+        straight = kv_all[pl.ds(2 * tile, 2)].reshape(kt, rows)
+        return straight, pltpu.roll(straight.astype(f32), hd, 1).astype(bf)
+
     def step(i, carry):
         @pl.when(i == 1)
         def _():
@@ -292,35 +321,10 @@
             def _():
                 kv_copy(kv_other, src, 0, lax.rem(y + 1, NY)).wait_recv()
 
-        straight = kv_all[pl.ds(2 * tile, 2)].reshape(kt, rows)
-        turned = pltpu.roll(straight.astype(f32), hd, 1).astype(bf)
-        for m in range(n_mb):
-            part = slice(m * mb, (m + 1) * mb)
-            per = mb // rows
-            queries = q_all[m * per : (m + 1) * per].reshape(mb, rows).astype(f32)
-            outs = []
-            sums = []
-            for u in range(2):
-                qh = jnp.where(jnp.logical_not(left2) if u else left2, queries, 0.0).astype(bf)
-                score = dot_t(qh, turned if u else straight) * scale + head_bias
-                pos = jnp.maximum(score, 0.0)
-                neg = score - pos
-                soft = jnp.log2(1.0 + jnp.exp2(neg - pos))
-                drop = pos + soft
-                hold = neg - soft
-                if m == 0:
-                    usable = (row2 >= rows) | (lane2 + tile * kt < place + u * half)
-                    drop = jnp.where(usable, drop, 0.0)
-                    hold = jnp.where(usable, hold, -jnp.inf)
-                suffix = dot(drop.astype(bf), later)
-                weights = jnp.exp2(hold - suffix).astype(bf)
-                outs.append(dot(weights, straight if u else turned))
-                sums.append(suffix[:, :1] + drop[:, :1])
-            o_seg[tile, part] = jnp.where(left2, outs[0], outs[1])
-            t_seg[tile, part] = jnp.where(left2, sums[0], sums[1])
+        straight, turned = keys_of(tile)
+        for m in range(2):
+            segment(m, tile, straight, turned)
         return carry
-
-    lax.fori_loop(0, NY // 2, step, 0)
 
     def to_owner(j, e, sp, which):
         if which:
@@ -328,7 +332,8 @@
         return remote(t_send.at[j], t_recv.at[j, e], t_ss.at[j, e], t_rs.at[j, e], sp, t)
 
     first = lax.broadcasted_iota(jnp.int32, (8, rows), 0) < 4
-    for j in range(NZ - 1, -1, -1):
+
+    def finish(j):
         part = slice(j * rows, (j + 1) * rows)
         last = NY // 2 - 1
         acc = o_seg[last, part]
@@ -341,8 +346,6 @@
         o_send[j] = acc.astype(bf).reshape(2, half, rows)
         t_send[j] = compact
         if j == 0:
-            own_t = compact
-            own_o = acc[:half]
             for which in range(2):
                 start(to_owner(0, 1, z * NY + y_other, which))
         else:
@@ -351,6 +354,23 @@
                 for e in range(2):
                     for which in range(2):
                         to_owner(j, e, (z + j) * NY + (y_other if e else y), which).start()
+        return acc[:half], compact
+
+    q_waits((0, 1, 2, 3))
+    lax.fori_loop(0, NY // 2, step, 0)
+    for j in (3, 2, 1, 0):
+        own_o, own_t = finish(j)
+    for m in (2, 3):
+        q_waits((2 * m, 2 * m + 1))
+
+        def far_step(i, carry):
+            for u in range(2):
+                segment(m, 2 * i + u, *keys_of(2 * i + u))
+            return carry
+
+        lax.fori_loop(0, NY // 4, far_step, 0)
+        for j in (2 * m, 2 * m + 1):
+            finish(j)
 
     def from_owner(j, e, which):
         frm = lax.rem(z + NZ - j, NZ) * NY + (y_other if e else y)

time: 58.6 us -> 51.1 us (0.87)
  Pallas kernels: 56.5 us -> 49.3 us
    pallas_call x1, Pallas kernels: 56.5 us -> 49.3 us  [one_kernel(): pl.pallas_call(kernel, out_shape=jax.ShapeDtypeStruct((cut, feats), bf),...]
where the time goes in v3:
time: 51.1 us; the launch traced here: 50.7 us
  Pallas kernels  49.3 us (96%)
  local copies, waits for them, and re-layouts  1.47 us (3%)
    pallas_call x1, Pallas kernels, one_kernel(): pl.pallas_call(kernel, out_shape=jax.ShapeDtypeStruct((cut, feats), bf),...  49.3 us
    unnamed x1, local copies, waits for them, and re-layouts  1.47 us

profile of v3, /device:TPU:1, one launch (start us, length us, event | category | flops | bytes accessed | tf_op | source)
XLA Modules:
  0.0 50.7 jit_solution(7945192262719975252)
XLA Ops:
  0.0 49.3 %layer.1 = bf16[16,2048]{1,0:T(8,128)(2,1)} custom-call(bf16[128,256]{1,0:T(8,128)(2,1)} %tokens.1, f32[2048]{0:T(1024)} %pre_gain_in.1, bf16[2048,128]{1,0:T(8,128)(2,1)} %wqs.1, bf16[2048,128]{1,0:T(8,128)(2,1)} %wks.1, bf16[2048,128]{1,0:T(8,128)(2,1)} %wvs.1, bf16[2048,128]{1,0:T(8,128)(2,1)} %wqw.1, bf16[64,2048]{1,0:T(8,128)(2,1)} %bitcast.2, ...), custom_call_target="tpu_custom_call" | custom-call | tf_op jit(solution)/shard_map/layer/pallas_call | solution.py:468
  49.3 1.5 %copy.17 = bf16[16,2048]{1,0:T(8,128)(2,1)} copy(bf16[16,2048]{1,0:T(8,128)(2,1)} %layer.1) | data formatting | bytes 131072

commit v4 on v3

--- a/solution.py
+++ b/solution.py
@@ -17,6 +17,7 @@
 NT = 8
 NX = 4
 N_SP = NY * NZ
+PLACE = (0, 1, 3, 5, 7, 6, 4, 2)
 
 
 def dot(a, b):
@@ -32,9 +33,9 @@
     post_gain_in, out,
     pre_gain, bias, sinks, sgain, wgain, post_gain, x, sq_acc, normed, vqs, vkv, vqw, vkvw, vos, vow,
     kv_all, kv_other, q_all, q_other, o_seg, t_seg, kvw, qw_buf, kvw_prev, o_send, o_recv, t_send, t_recv,
-    a_send, a_recv, b_send, b_recv, total,
+    a_send, a_recv, b_send, b_recv, total, out_buf,
     w_sem, tok_sem, x_ss, x_rs, kv_ss, kv_rs, q_ss, q_rs, p_ss, p_rs, o_ss, o_rs, t_ss, t_rs,
-    a_ss, a_rs, b_ss, b_rs,
+    a_ss, a_rs, b_ss, b_rs, out_sem,
 ):
     bf = jnp.bfloat16
     f32 = jnp.float32
@@ -86,7 +87,7 @@
     for j in range(1, NZ):
         @pl.when(z + j >= NZ)
         def _():
-            q_all[j] = jnp.zeros((2, half, rows), bf)
+            q_all[PLACE[j]] = jnp.zeros((2, half, rows), bf)
 
         @pl.when(z - j < 0)
         def _():
@@ -155,7 +156,7 @@
     def kv_send(k):
         start(kv_copy(kv_other if k % 2 else kv_all.at[y], y, k, lax.rem(y + k, NY)))
 
-    for k in (1, 7, 2, 6):
+    for k in (1, 7):
         kv_send(k)
 
     l_qs.wait()
@@ -168,11 +169,11 @@
     def q_copy(j, e, to_z):
         src = q_other if e else q_all.at[0, 0]
         return remote(
-            src, q_all.at[j, e], q_ss.at[j, e], q_rs.at[j, e], to_z * NY + (y_other if e else y), t
+            src, q_all.at[PLACE[j], e], q_ss.at[j, e], q_rs.at[j, e], to_z * NY + (y_other if e else y), t
         )
 
     start(q_copy(0, 1, z))
-    for j in (1, 2, 3, 4, 5, 6, 7):
+    for j in (1, 7, 2, 6, 3, 5, 4):
         @pl.when(z - j >= 0)
         def _():
             q_copy(j, 0, z - j).start()
@@ -189,7 +190,7 @@
     def _():
         prev_copy(s + 1).start()
 
-    for k in (3, 5, 4):
+    for k in (2, 6, 3, 5, 4):
         kv_send(k)
 
     @pl.when(s == 0)
@@ -257,7 +258,7 @@
 
     def q_wait(j, e):
         frm = lax.rem(z + j, NZ) * NY + (y_other if e else y)
-        remote(q_other, q_all.at[j, e], q_ss.at[j, e], q_rs.at[j, e], frm, t).wait_recv()
+        remote(q_other, q_all.at[PLACE[j], e], q_ss.at[j, e], q_rs.at[j, e], frm, t).wait_recv()
 
     def q_waits(js):
         for j in js:
@@ -280,8 +281,9 @@
     scale = LOG2E * hd**-0.5
     head_bias = bias[head] * LOG2E
 
-    def segment(m, tile, straight, turned):
+    def segment(m, tile):
         part = slice(m * mb, (m + 1) * mb)
+        straight, turned = keys_of(tile)
         queries = q_all[m * per : (m + 1) * per].reshape(mb, rows).astype(f32)
         outs = []
         sums = []
@@ -308,23 +310,17 @@
         straight = kv_all[pl.ds(2 * tile, 2)].reshape(kt, rows)
         return straight, pltpu.roll(straight.astype(f32), hd, 1).astype(bf)
 
-    def step(i, carry):
-        @pl.when(i == 1)
-        def _():
-            windowed()
-
-        tile = lax.rem(y // 2 + i + i // 2 - 2 * (i // 3), NY // 2)
+    near = y // 2
+    side = 2 * head - 1
+    tiles = [lax.rem(near + k * side + NY // 2, NY // 2) for k in (0, 1, -1, 2)]
+
+    def kv_waits(k):
         for u in range(2):
-            src = 2 * tile + u
+            src = 2 * tiles[k] + u
 
             @pl.when(src != y)
             def _():
                 kv_copy(kv_other, src, 0, lax.rem(y + 1, NY)).wait_recv()
-
-        straight, turned = keys_of(tile)
-        for m in range(2):
-            segment(m, tile, straight, turned)
-        return carry
 
     def to_owner(j, e, sp, which):
         if which:
@@ -334,7 +330,7 @@
     first = lax.broadcasted_iota(jnp.int32, (8, rows), 0) < 4
 
     def finish(j):
-        part = slice(j * rows, (j + 1) * rows)
+        part = slice(PLACE[j] * rows, (PLACE[j] + 1) * rows)
         last = NY // 2 - 1
         acc = o_seg[last, part]
         carry = t_seg[last, part]
@@ -356,21 +352,35 @@
                         to_owner(j, e, (z + j) * NY + (y_other if e else y), which).start()
         return acc[:half], compact
 
-    q_waits((0, 1, 2, 3))
-    lax.fori_loop(0, NY // 2, step, 0)
-    for j in (3, 2, 1, 0):
-        own_o, own_t = finish(j)
-    for m in (2, 3):
-        q_waits((2 * m, 2 * m + 1))
-
-        def far_step(i, carry):
-            for u in range(2):
-                segment(m, 2 * i + u, *keys_of(2 * i + u))
-            return carry
-
-        lax.fori_loop(0, NY // 4, far_step, 0)
-        for j in (2 * m, 2 * m + 1):
-            finish(j)
+    def segments(*pairs):
+        for m, k in pairs:
+            segment(m, tiles[k])
+
+    q_waits((0, 1))
+    kv_waits(0)
+    segments((0, 0))
+    windowed()
+    q_waits((7, 2))
+    kv_waits(1)
+    segments((0, 1), (1, 0))
+    segments((1, 1))
+    q_waits((6, 3))
+    segments((2, 0), (2, 1))
+    kv_waits(2)
+    segments((0, 2), (1, 2))
+    kv_waits(3)
+    segments((0, 3), (1, 3))
+    own_o, own_t = finish(0)
+    for j in (2, 1, 7):
+        finish(j)
+    segments((2, 2), (2, 3))
+    for j in (3, 6):
+        finish(j)
+    q_waits((5, 4))
+    segments((3, 0), (3, 1))
+    segments((3, 2), (3, 3))
+    for j in (4, 5):
+        finish(j)
 
     def from_owner(j, e, which):
         frm = lax.rem(z + NZ - j, NZ) * NY + (y_other if e else y)
@@ -415,8 +425,10 @@
     inv_s = take(a_send, a_recv, a_ss, a_rs, total.at[0], NT * rows)
     both = (total[0] * inv_s + total[1]).astype(bf).astype(f32)
     stats = jnp.sum(both * both, axis=1, keepdims=True) * (1.0 / feats)
-    out[...] = (both * lax.rsqrt(stats + EPS) * post_gain[...].reshape(1, feats)).astype(bf)
-
+    out_buf[...] = (both * lax.rsqrt(stats + EPS) * post_gain[...].reshape(1, feats)).astype(bf)
+
+    out_copy = pltpu.make_async_copy(out_buf, out, out_sem)
+    out_copy.start()
     for refs in ((a_send, a_recv, a_ss, a_rs), (b_send, b_recv, b_ss, b_rs)):
         for copy in given(*refs):
             copy.wait_send()
@@ -437,6 +449,8 @@
     def _():
         prev_copy(s + 1).wait_send()
 
+    out_copy.wait()
+
 
 def one_kernel(*args):
     tokens, pre_gain, wqs, wks, wvs, wqw, wkw, wvw, bias, sinks, sgain, wgain, wos, wow, post_gain = args
@@ -448,7 +462,6 @@
     v = pltpu.VMEM
     dma = pltpu.SemaphoreType.DMA
     anywhere = pl.BlockSpec(memory_space=pl.ANY)
-    vmem = pl.BlockSpec(memory_space=pltpu.VMEM)
     scratch = [
         v(pre_gain.shape, f32), pltpu.SMEM(bias.shape, f32), pltpu.SMEM(sinks.shape, f32),
         v(sgain.shape, f32), v(wgain.shape, f32), v(post_gain.shape, f32),
@@ -461,15 +474,15 @@
         v((NZ, 2, rows // 2, rows), bf), v((NZ, 2, rows // 2, rows), bf),
         v((NZ, 8, rows), f32), v((NZ, 2, 8, rows), f32),
         v((NT, cut, feats + rows), bf), v((NT, cut, feats + rows), bf),
-        v((NT, cut, feats + rows), bf), v((NT, cut, feats + rows), bf), v((2, cut, feats), f32),
+        v((NT, cut, feats + rows), bf), v((NT, cut, feats + rows), bf), v((2, cut, feats), f32), v((cut, feats), bf),
         dma((14,)), dma, dma((8,)), dma((NT,)), dma((NY,)), dma((NY,)), dma((NZ, 2)), dma((NZ, 2)), dma, dma,
-        dma((NZ, 2)), dma((NZ, 2)), dma((NZ, 2)), dma((NZ, 2)), dma((NT,)), dma((NT,)), dma((NT,)), dma((NT,)),
+        dma((NZ, 2)), dma((NZ, 2)), dma((NZ, 2)), dma((NZ, 2)), dma((NT,)), dma((NT,)), dma((NT,)), dma((NT,)), dma,
     ]
     return pl.pallas_call(
         kernel,
         out_shape=jax.ShapeDtypeStruct((cut, feats), bf),
         in_specs=[anywhere] * len(args),
-        out_specs=vmem,
+        out_specs=anywhere,
         scratch_shapes=scratch,
         compiler_params=pltpu.CompilerParams(
             collective_id=0, has_side_effects=True, vmem_limit_bytes=67043328

time: 51.1 us -> 50.4 us (0.986)
  Pallas kernels: 49.3 us -> 48.3 us
    pallas_call x1, Pallas kernels: 49.3 us -> 48.3 us  [one_kernel(): pl.pallas_call(kernel, out_shape=jax.ShapeDtypeStruct((cut, feats), bf),...]
where the time goes in v4:
time: 50.4 us; the launch traced here: 49.7 us
  Pallas kernels  48.3 us (96%)
  local copies, waits for them, and re-layouts  1.47 us (3%)
    pallas_call x1, Pallas kernels, one_kernel(): pl.pallas_call(kernel, out_shape=jax.ShapeDtypeStruct((cut, feats), bf),...  48.3 us
    unnamed x1, local copies, waits for them, and re-layouts  1.47 us

profile of v4, /device:TPU:1, one launch (start us, length us, event | category | flops | bytes accessed | tf_op | source)
XLA Modules:
  0.0 49.7 jit_solution(17000008929499100943)
XLA Ops:
  0.0 48.3 %layer.1 = bf16[16,2048]{1,0:T(8,128)(2,1)} custom-call(bf16[128,256]{1,0:T(8,128)(2,1)} %tokens.1, f32[2048]{0:T(1024)} %pre_gain_in.1, bf16[2048,128]{1,0:T(8,128)(2,1)} %wqs.1, bf16[2048,128]{1,0:T(8,128)(2,1)} %wks.1, bf16[2048,128]{1,0:T(8,128)(2,1)} %wvs.1, bf16[2048,128]{1,0:T(8,128)(2,1)} %wqw.1, bf16[64,2048]{1,0:T(8,128)(2,1)} %bitcast.2, ...), custom_call_target="tpu_custom_call" | custom-call | tf_op jit(solution)/shard_map/layer/pallas_call | solution.py:481
  48.3 1.5 %copy.17 = bf16[16,2048]{1,0:T(8,128)(2,1)} copy(bf16[16,2048]{1,0:T(8,128)(2,1)} %layer.1) | data formatting | bytes 131072

commit v5 on v4

--- a/solution.py
+++ b/solution.py
@@ -31,11 +31,12 @@
 def kernel(
     tokens, pre_gain_in, wqs, wks, wvs, wqw, wkw, wvw, bias_in, sinks_in, sgain_in, wgain_in, wos, wow,
     post_gain_in, out,
-    pre_gain, bias, sinks, sgain, wgain, post_gain, x, sq_acc, normed, vqs, vkv, vqw, vkvw, vos, vow,
+    pre_gain, bias, sinks, sgain, wgain, post_gain, x, sq_acc, proj, vproj, kvw_acc, vkvw, vos, vow,
     kv_all, kv_other, q_all, q_other, o_seg, t_seg, kvw, qw_buf, kvw_prev, o_send, o_recv, t_send, t_recv,
-    a_send, a_recv, b_send, b_recv, total, out_buf,
+    a_keep0, a_keep1, d_send0, d_send1, d_recv0, d_recv1, r_send0, r_send1, r_recv0, r_recv1,
+    b_send, b_recv, total, out_buf,
     w_sem, tok_sem, x_ss, x_rs, kv_ss, kv_rs, q_ss, q_rs, p_ss, p_rs, o_ss, o_rs, t_ss, t_rs,
-    a_ss, a_rs, b_ss, b_rs, out_sem,
+    d_ss, d_rs, r_ss, r_rs, b_ss, b_rs, out_sem,
 ):
     bf = jnp.bfloat16
     f32 = jnp.float32
@@ -72,13 +73,15 @@
     loads = [
         pltpu.make_async_copy(src, dst, w_sem.at[n])
         for n, (src, dst) in enumerate(
-            [(wks, vkv.at[:, :rows]), (wvs, vkv.at[:, rows:]), (wqs, vqs), (wkw, vkvw.at[:half]), (wvw, vkvw.at[half:]), (wqw, vqw),
+            [(wks, vproj.at[:, :rows]), (wvs, vproj.at[:, rows : 2 * rows]), (wqs, vproj.at[:, 2 * rows : 3 * rows]),
+             (wqw, vproj.at[:, 3 * rows :]), (wkw, vkvw.at[:half]), (wvw, vkvw.at[half:]),
              (wow, vow), (wos, vos),
              (bias_in, bias), (pre_gain_in, pre_gain), (sinks_in, sinks), (sgain_in, sgain),
              (wgain_in, wgain), (post_gain_in, post_gain)]
         )
     ]
-    l_ks, l_vs, l_qs, l_kw, l_vw, l_qw, l_ow, l_os, *l_small = loads
+    l_proj = loads[:6]
+    l_ow, l_os, *l_small = loads[6:]
     tok_load = pltpu.make_async_copy(tokens, x.at[t], tok_sem)
     tok_load.start()
     for load in l_small + loads[:8]:
@@ -118,33 +121,33 @@
         start(x_copy(t, dx, lax.rem(chip + dx, NX) * 2 + core))
     start(x_copy(t, 0, partner))
 
-    def squares(slot):
+    def absorb(slot, first=False):
         v = x[slot].astype(f32)
+        part = pl.ds(pl.multiple_of(slot * chunk, chunk), chunk)
+        gained = (v * pre_gain[part].reshape(1, chunk)).astype(bf)
         v = v * v
-        return v[:, : chunk // 2] + v[:, chunk // 2 :]
-
-    sq_acc[...] = squares(t)
-    for dx in (1, 3, 2):
-        slot = lax.rem(chip + NX - dx, NX) * 2 + core
+        v = v[:, : chunk // 2] + v[:, chunk // 2 :]
+        sq_acc[...] = v if first else sq_acc[...] + v
+        more = dot(gained, vproj[part, :])
+        proj[...] = more if first else proj[...] + more
+        more = dot_t(gained, vkvw[:, part])
+        kvw_acc[...] = more if first else kvw_acc[...] + more
+
+    for load in l_proj:
+        load.wait()
+    absorb(t, True)
+    for dx, relayed in ((0, 1), (1, 0), (3, 0), (1, 1), (3, 1), (2, 0), (2, 1)):
+        slot = lax.rem(chip + NX - dx, NX) * 2 + (1 - core if relayed else core)
         x_copy(slot, dx, partner).wait_recv()
-        start(x_copy(slot, NX + dx, partner))
-        sq_acc[...] += squares(slot)
-    for dx in (0, 1, 3, 2):
-        slot = lax.rem(chip + NX - dx, NX) * 2 + 1 - core
-        x_copy(slot, dx, partner).wait_recv()
-        sq_acc[...] += squares(slot)
+        if not relayed:
+            start(x_copy(slot, NX + dx, partner))
+        absorb(slot)
     inv = lax.rsqrt(jnp.sum(sq_acc[...], axis=1, keepdims=True) * (1.0 / feats) + EPS)
-    for k in range(NT):
-        cols = slice(k * chunk, (k + 1) * chunk)
-        normed[:, cols] = (x[k].astype(f32) * inv * pre_gain[cols].reshape(1, chunk)).astype(bf)
 
     left = lax.broadcasted_iota(jnp.int32, (rows, rows), 1) < hd
     left_half = left[:half]
 
-    l_ks.wait()
-    l_vs.wait()
-    kv = dot(normed[...], vkv[...])
-    keys, values = kv[:, :rows], kv[:, rows:]
+    keys, values = proj[:, :rows] * inv, proj[:, rows : 2 * rows] * inv
     head0 = jnp.where(left, keys, pltpu.roll(values, hd, 1))
     head1 = jnp.where(left, pltpu.roll(keys, hd, 1), values)
     kv_all[y] = jnp.where(head == 0, head0, head1).astype(bf)
@@ -159,8 +162,7 @@
     for k in (1, 7):
         kv_send(k)
 
-    l_qs.wait()
-    qs = dot(normed[...], vqs[...])
+    qs = proj[:, 2 * rows : 3 * rows] * inv
     q0 = jnp.where(left_half, qs[:half], pltpu.roll(qs[half:], hd, 1))
     q1 = jnp.where(left_half, pltpu.roll(qs[:half], hd, 1), qs[half:])
     q_all[0, 0] = jnp.where(head == 0, q0, q1).astype(bf)
@@ -179,9 +181,7 @@
             q_copy(j, 0, z - j).start()
             q_copy(j, 1, z - j).start()
 
-    l_kw.wait()
-    l_vw.wait()
-    kvw[...] = dot_t(normed[...], vkvw[...]).astype(bf)
+    kvw[...] = (kvw_acc[...] * inv).astype(bf)
 
     def prev_copy(to):
         return remote(kvw, kvw_prev, p_ss, p_rs, to, t)
@@ -197,8 +197,7 @@
     def _():
         kvw_prev[...] = jnp.zeros_like(kvw_prev)
 
-    l_qw.wait()
-    qw_buf[...] = dot(normed[...], vqw[...])
+    qw_buf[...] = proj[:, 3 * rows :] * inv
 
     def given(send, recv, ss, rs):
         for dx, dc in ((2, 0), (2, 1), (1, 0), (1, 1), (3, 0), (3, 1), (0, 1)):
@@ -281,30 +280,53 @@
     scale = LOG2E * hd**-0.5
     head_bias = bias[head] * LOG2E
 
-    def segment(m, tile):
-        part = slice(m * mb, (m + 1) * mb)
-        straight, turned = keys_of(tile)
-        queries = q_all[m * per : (m + 1) * per].reshape(mb, rows).astype(f32)
-        outs = []
-        sums = []
-        for u in range(2):
-            qh = jnp.where(jnp.logical_not(left2) if u else left2, queries, 0.0).astype(bf)
-            score = dot_t(qh, turned if u else straight) * scale + head_bias
+    def segment(pairs):
+        weights_of = {}
+        chains = []
+        for m, k in pairs:
+            if k not in weights_of:
+                weights_of[k] = keys_of(tiles[k])
+            queries = q_all[m * per : (m + 1) * per].reshape(mb, rows).astype(f32)
+            for u in range(2):
+                qh = jnp.where(jnp.logical_not(left2) if u else left2, queries, 0.0).astype(bf)
+                chains.append((m, k, u, qh))
+
+        def by_weights(values, flip):
+            res = [None] * len(chains)
+            for k in weights_of:
+                for u in range(2):
+                    own = [n for n, c in enumerate(chains) if c[1] == k and c[2] == u]
+                    joint = jnp.concatenate([values[n] for n in own], axis=0)
+                    w = weights_of[k][1 - u if flip else u]
+                    got = dot(joint, w) if flip else dot_t(joint, w)
+                    for at, n in enumerate(own):
+                        res[n] = got[at * mb : (at + 1) * mb]
+            return res
+
+        drops = []
+        holds = []
+        for (m, k, u, _), raw in zip(chains, by_weights([c[3] for c in chains], False)):
+            score = raw * scale + head_bias
             pos = jnp.maximum(score, 0.0)
             neg = score - pos
             soft = jnp.log2(1.0 + jnp.exp2(neg - pos))
             drop = pos + soft
             hold = neg - soft
             if m == 0:
-                usable = (row2 >= rows) | (lane2 + tile * kt < place + u * half)
+                usable = (row2 >= rows) | (lane2 + tiles[k] * kt < place + u * half)
                 drop = jnp.where(usable, drop, 0.0)
                 hold = jnp.where(usable, hold, -jnp.inf)
-            suffix = dot(drop.astype(bf), later)
-            weights = jnp.exp2(hold - suffix).astype(bf)
-            outs.append(dot(weights, straight if u else turned))
-            sums.append(suffix[:, :1] + drop[:, :1])
-        o_seg[tile, part] = jnp.where(left2, outs[0], outs[1])
-        t_seg[tile, part] = jnp.where(left2, sums[0], sums[1])
+            drops.append(drop)
+            holds.append(hold)
+        suffix = dot(jnp.concatenate([d.astype(bf) for d in drops], axis=0), later)
+        suffix = [suffix[n * mb : (n + 1) * mb] for n in range(len(chains))]
+        outs = by_weights([jnp.exp2(h - f).astype(bf) for h, f in zip(holds, suffix)], True)
+        sums = [f[:, :1] + d[:, :1] for f, d in zip(suffix, drops)]
+        for n in range(0, len(chains), 2):
+            m, k, _, _ = chains[n]
+            part = slice(m * mb, (m + 1) * mb)
+            o_seg[tiles[k], part] = jnp.where(left2, outs[n], outs[n + 1])
+            t_seg[tiles[k], part] = jnp.where(left2, sums[n], sums[n + 1])
 
     def keys_of(tile):
         straight = kv_all[pl.ds(2 * tile, 2)].reshape(kt, rows)
@@ -353,8 +375,7 @@
         return acc[:half], compact
 
     def segments(*pairs):
-        for m, k in pairs:
-            segment(m, tiles[k])
+        segment(pairs)
 
     q_waits((0, 1))
     kv_waits(0)
@@ -362,25 +383,22 @@
     windowed()
     q_waits((7, 2))
     kv_waits(1)
-    segments((0, 1), (1, 0))
-    segments((1, 1))
-    q_waits((6, 3))
-    segments((2, 0), (2, 1))
+    segments((0, 1), (1, 1))
+    segments((1, 0))
+    q_waits((6, 3, 5, 4))
+    segments((2, 0), (3, 0))
+    segments((2, 1), (3, 1))
     kv_waits(2)
+    segments((2, 2), (3, 2))
+    kv_waits(3)
+    segments((2, 3), (3, 3))
+    for j in (4, 5, 3, 6):
+        finish(j)
     segments((0, 2), (1, 2))
-    kv_waits(3)
     segments((0, 3), (1, 3))
-    own_o, own_t = finish(0)
     for j in (2, 1, 7):
         finish(j)
-    segments((2, 2), (2, 3))
-    for j in (3, 6):
-        finish(j)
-    q_waits((5, 4))
-    segments((3, 0), (3, 1))
-    segments((3, 2), (3, 3))
-    for j in (4, 5):
-        finish(j)
+    own_o, own_t = finish(0)
 
     def from_owner(j, e, which):
         frm = lax.rem(z + NZ - j, NZ) * NY + (y_other if e else y)
@@ -418,20 +436,70 @@
         axis=0,
     ).astype(bf).astype(f32)
     l_os.wait()
-    give(a_send, a_recv, a_ss, a_rs, s_out, ((s_out * sgain[...].reshape(1, rows)).astype(bf), vos))
-
+    gained = (s_out * sgain[...].reshape(1, rows)).astype(bf)
+    own_sums = jnp.broadcast_to(jnp.sum(s_out * s_out, axis=1, keepdims=True), (rows, rows))
+    part = feats // 2
+    pieces = ((a_keep0, d_send0, d_recv0, r_send0, r_recv0), (a_keep1, d_send1, d_recv1, r_send1, r_recv1))
+    left_cut = left[:cut].reshape(1, cut, rows)
+
+    def halves(values):
+        return jnp.where(core == 0, values[:, 0], values[:, 1]), jnp.where(core == 0, values[:, 1], values[:, 0])
+
+    def in_two(values):
+        high = values.astype(bf).astype(f32)
+        return jnp.where(left_cut, high, values - high).astype(bf)
+
+    def joined(values):
+        return values + pltpu.roll(values, hd, values.ndim - 1)
+
+    def across(n):
+        return remote(pieces[n][1], pieces[n][2], d_ss.at[n], d_rs.at[n], s, partner)
+
+    def along(n, dx):
+        to = lax.rem(chip + dx, NX)
+        return remote(
+            pieces[n][3].at[to], pieces[n][4].at[chip], r_ss.at[n, dx], r_rs.at[n, chip], s, to * 2 + core
+        )
+
+    for n, (keep, d_send, _, _, _) in enumerate(pieces):
+        mine, theirs = halves(dot(gained, vos[:, n * part : (n + 1) * part]).reshape(NX, 2, cut, part))
+        keep[:, :, :part] = mine
+        d_send[:, :, :part] = theirs.astype(bf)
+        if n == 0:
+            mine, theirs = halves(own_sums.reshape(NX, 2, cut, rows))
+            keep[:, :, part:] = mine
+            d_send[:, :, part:] = in_two(theirs)
+        start(across(n))
     inv_w = take(b_send, b_recv, b_ss, b_rs, total.at[1], NT * rows)
     total[1] = total[1] * inv_w
-    inv_s = take(a_send, a_recv, a_ss, a_rs, total.at[0], NT * rows)
+    for n, (keep, _, d_recv, r_send, _) in enumerate(pieces):
+        across(n).wait_recv()
+        r_send[:, :, :part] = (keep[:, :, :part] + d_recv[:, :, :part].astype(f32)).astype(bf)
+        if n == 0:
+            r_send[:, :, part:] = in_two(keep[:, :, part:] + joined(d_recv[:, :, part:].astype(f32)))
+        for dx in (2, 1, 3):
+            start(along(n, dx))
+    sums = None
+    for n, (_, _, _, r_send, r_recv) in enumerate(pieces):
+        got = r_send[chip].astype(f32)
+        for dx in (1, 3, 2):
+            frm = lax.rem(chip + dx, NX)
+            remote(
+                r_send.at[frm], r_recv.at[frm], r_ss.at[n, dx], r_rs.at[n, frm], s, partner
+            ).wait_recv()
+            got = got + r_recv[frm].astype(f32)
+        total[0, :, n * part : (n + 1) * part] = got[:, :part]
+        if n == 0:
+            sums = joined(got[:, part:])
+    inv_s = lax.rsqrt(sums[:, :1] * (1.0 / (NT * rows)) + EPS)
     both = (total[0] * inv_s + total[1]).astype(bf).astype(f32)
     stats = jnp.sum(both * both, axis=1, keepdims=True) * (1.0 / feats)
     out_buf[...] = (both * lax.rsqrt(stats + EPS) * post_gain[...].reshape(1, feats)).astype(bf)
 
     out_copy = pltpu.make_async_copy(out_buf, out, out_sem)
     out_copy.start()
-    for refs in ((a_send, a_recv, a_ss, a_rs), (b_send, b_recv, b_ss, b_rs)):
-        for copy in given(*refs):
-            copy.wait_send()
+    for copy in given(b_send, b_recv, b_ss, b_rs):
+        copy.wait_send()
     for copy in sends:
         copy.wait_send()
     for j in range(1, NZ):
@@ -459,24 +527,26 @@
     rows, chunk = tokens.shape
     feats = NT * chunk
     cut = rows // NT
+    widths = (feats // 2 + rows, feats // 2)
     v = pltpu.VMEM
     dma = pltpu.SemaphoreType.DMA
     anywhere = pl.BlockSpec(memory_space=pl.ANY)
     scratch = [
         v(pre_gain.shape, f32), pltpu.SMEM(bias.shape, f32), pltpu.SMEM(sinks.shape, f32),
         v(sgain.shape, f32), v(wgain.shape, f32), v(post_gain.shape, f32),
-        v((NT, rows, chunk), bf), v((rows, rows), f32), v((rows, feats), bf),
-        v(wqs.shape, bf), v((feats, 2 * rows), bf), v(wqw.shape, bf), v((rows, feats), bf),
+        v((NT, rows, chunk), bf), v((rows, rows), f32), v((rows, 4 * rows), f32), v((feats, 4 * rows), bf),
+        v((rows, rows), f32), v((rows, feats), bf),
         v(wos.shape, bf), v(wow.shape, bf),
         v((NY, rows, rows), bf), v((rows, rows), bf), v((NZ, 2, rows // 2, rows), bf), v((rows // 2, rows), bf),
         v((NY // 2, NZ * rows, rows), f32), v((NY // 2, NZ * rows, rows), f32),
         v((rows, rows), bf), v((rows, rows), f32), v((rows, rows), bf),
         v((NZ, 2, rows // 2, rows), bf), v((NZ, 2, rows // 2, rows), bf),
         v((NZ, 8, rows), f32), v((NZ, 2, 8, rows), f32),
-        v((NT, cut, feats + rows), bf), v((NT, cut, feats + rows), bf),
+        *(v((NX, cut, width), f32) for width in widths),
+        *(v((NX, cut, width), bf) for _ in range(4) for width in widths),
         v((NT, cut, feats + rows), bf), v((NT, cut, feats + rows), bf), v((2, cut, feats), f32), v((cut, feats), bf),
         dma((14,)), dma, dma((8,)), dma((NT,)), dma((NY,)), dma((NY,)), dma((NZ, 2)), dma((NZ, 2)), dma, dma,
-        dma((NZ, 2)), dma((NZ, 2)), dma((NZ, 2)), dma((NZ, 2)), dma((NT,)), dma((NT,)), dma((NT,)), dma((NT,)), dma,
+        dma((NZ, 2)), dma((NZ, 2)), dma((NZ, 2)), dma((NZ, 2)), dma((2,)), dma((2,)), dma((2, NX)), dma((2, NX)), dma((NT,)), dma((NT,)), dma,
     ]
     return pl.pallas_call(
         kernel,

time: 50.4 us -> 50.6 us (level)
  Pallas kernels: 48.3 us -> 49 us
    pallas_call x1, Pallas kernels: 48.3 us -> 49 us  [one_kernel(): pl.pallas_call(kernel, out_shape=jax.ShapeDtypeStruct((cut, feats), bf),...]
where the time goes in v5:
time: 50.6 us; the launch traced here: 50.4 us
  Pallas kernels  49 us (97%)
  local copies, waits for them, and re-layouts  1.47 us (3%)
    pallas_call x1, Pallas kernels, one_kernel(): pl.pallas_call(kernel, out_shape=jax.ShapeDtypeStruct((cut, feats), bf),...  49 us
    unnamed x1, local copies, waits for them, and re-layouts  1.47 us

profile of v5, /device:TPU:1, one launch (start us, length us, event | category | flops | bytes accessed | tf_op | source)
XLA Modules:
  0.0 50.4 jit_solution(6819511070184481390)
XLA Ops:
  0.0 49.0 %layer.1 = bf16[16,2048]{1,0:T(8,128)(2,1)} custom-call(bf16[128,256]{1,0:T(8,128)(2,1)} %tokens.1, f32[2048]{0:T(1024)} %pre_gain_in.1, bf16[2048,128]{1,0:T(8,128)(2,1)} %wqs.1, bf16[2048,128]{1,0:T(8,128)(2,1)} %wks.1, bf16[2048,128]{1,0:T(8,128)(2,1)} %wvs.1, bf16[2048,128]{1,0:T(8,128)(2,1)} %wqw.1, bf16[64,2048]{1,0:T(8,128)(2,1)} %bitcast.2, ...), custom_call_target="tpu_custom_call" | custom-call | tf_op jit(solution)/shard_map/layer/pallas_call | solution.py:551
  49.0 1.5 %copy.17 = bf16[16,2048]{1,0:T(8,128)(2,1)} copy(bf16[16,2048]{1,0:T(8,128)(2,1)} %layer.1) | data formatting | bytes 131072

commit v6 on v5

--- a/solution.py
+++ b/solution.py
@@ -17,7 +17,7 @@
 NT = 8
 NX = 4
 N_SP = NY * NZ
-PLACE = (0, 1, 3, 5, 7, 6, 4, 2)
+PLACE = (0, 1, 2, 3, 7, 6, 5, 4)
 
 
 def dot(a, b):
@@ -36,7 +36,7 @@
     a_keep0, a_keep1, d_send0, d_send1, d_recv0, d_recv1, r_send0, r_send1, r_recv0, r_recv1,
     b_send, b_recv, total, out_buf,
     w_sem, tok_sem, x_ss, x_rs, kv_ss, kv_rs, q_ss, q_rs, p_ss, p_rs, o_ss, o_rs, t_ss, t_rs,
-    d_ss, d_rs, r_ss, r_rs, b_ss, b_rs, out_sem,
+    d_ss, d_rs, r_ss, r_rs, b_ss, b_rs, out_sem, ready,
 ):
     bf = jnp.bfloat16
     f32 = jnp.float32
@@ -59,15 +59,21 @@
     def greet(sp, tp):
         pl.semaphore_signal(barrier, inc=1, device_id={"sp": sp, "tp": tp}, device_id_type=MESH)
 
-    for k in range(1, NZ):
-        greet(lax.rem(z + k, NZ) * NY + y, t)
-        greet(lax.rem(z + k, NZ) * NY + y_other, t)
+    for k in range(1, NT):
+        greet(s, lax.rem(t + k, NT))
     for k in range(1, NY):
         greet(z * NY + lax.rem(y + k, NY), t)
-    for k in range(1, NT):
-        greet(s, lax.rem(t + k, NT))
-    greet(lax.rem(s + 1, N_SP), t)
-    greet(lax.rem(s + N_SP - 1, N_SP), t)
+    for k in range(1, NZ):
+        @pl.when(z + k < NZ)
+        def _():
+            greet((z + k) * NY + y, t)
+            greet((z + k) * NY + y_other, t)
+    starts_row = jnp.logical_and(y == 0, z > 0)
+    ends_row = jnp.logical_and(y == NY - 1, z < NZ - 1)
+
+    @pl.when(ends_row)
+    def _():
+        greet(s + 1, t)
 
     half = rows // 2
     loads = [
@@ -100,7 +106,11 @@
     for load in l_small:
         load.wait()
     tok_load.wait()
-    pl.semaphore_wait(barrier, 2 * NZ + NY + NT - 4 + 2)
+    pl.semaphore_wait(barrier, NT - 1 + NY - 1 + 2 * z + starts_row.astype(jnp.int32))
+
+    @pl.when(starts_row)
+    def _():
+        pl.semaphore_signal(ready, inc=1, device_id={"sp": s - 1, "tp": t}, device_id_type=MESH)
 
     def remote(src, dst, ss, rs, sp, tp):
         return pltpu.make_async_remote_copy(
@@ -121,27 +131,32 @@
         start(x_copy(t, dx, lax.rem(chip + dx, NX) * 2 + core))
     start(x_copy(t, 0, partner))
 
-    def absorb(slot, first=False):
-        v = x[slot].astype(f32)
-        part = pl.ds(pl.multiple_of(slot * chunk, chunk), chunk)
-        gained = (v * pre_gain[part].reshape(1, chunk)).astype(bf)
-        v = v * v
-        v = v[:, : chunk // 2] + v[:, chunk // 2 :]
-        sq_acc[...] = v if first else sq_acc[...] + v
-        more = dot(gained, vproj[part, :])
-        proj[...] = more if first else proj[...] + more
-        more = dot_t(gained, vkvw[:, part])
-        kvw_acc[...] = more if first else kvw_acc[...] + more
-
-    for load in l_proj:
-        load.wait()
-    absorb(t, True)
-    for dx, relayed in ((0, 1), (1, 0), (3, 0), (1, 1), (3, 1), (2, 0), (2, 1)):
+    def absorb(*slots, first=False):
+        sums = None
+        for slot in slots:
+            v = x[slot].astype(f32)
+            part = pl.ds(pl.multiple_of(slot * chunk, chunk), chunk)
+            gained = (v * pre_gain[part].reshape(1, chunk)).astype(bf)
+            v = v * v
+            more = (
+                v[:, : chunk // 2] + v[:, chunk // 2 :], dot(gained, vproj[part, :]), dot_t(gained, vkvw[:, part])
+            )
+            sums = more if sums is None else tuple(p + q for p, q in zip(sums, more))
+        for ref, more in zip((sq_acc, proj, kvw_acc), sums):
+            ref[...] = more if first else ref[...] + more
+
+    def block(dx, relayed):
         slot = lax.rem(chip + NX - dx, NX) * 2 + (1 - core if relayed else core)
         x_copy(slot, dx, partner).wait_recv()
         if not relayed:
             start(x_copy(slot, NX + dx, partner))
-        absorb(slot)
+        return slot
+
+    for load in l_proj:
+        load.wait()
+    absorb(t, block(0, 1), first=True)
+    absorb(*[block(dx, 0) for dx in (1, 3, 2)])
+    absorb(*[block(dx, 1) for dx in (1, 3, 2)])
     inv = lax.rsqrt(jnp.sum(sq_acc[...], axis=1, keepdims=True) * (1.0 / feats) + EPS)
 
     left = lax.broadcasted_iota(jnp.int32, (rows, rows), 1) < hd
@@ -186,12 +201,17 @@
     def prev_copy(to):
         return remote(kvw, kvw_prev, p_ss, p_rs, to, t)
 
-    @pl.when(s < N_SP - 1)
+    @pl.when(y < NY - 1)
     def _():
         prev_copy(s + 1).start()
 
     for k in (2, 6, 3, 5, 4):
         kv_send(k)
+
+    @pl.when(ends_row)
+    def _():
+        pl.semaphore_wait(ready, 1)
+        prev_copy(s + 1).start()
 
     @pl.when(s == 0)
     def _():
@@ -381,24 +401,27 @@
     kv_waits(0)
     segments((0, 0))
     windowed()
-    q_waits((7, 2))
     kv_waits(1)
+    q_waits((2, 3))
     segments((0, 1), (1, 1))
     segments((1, 0))
-    q_waits((6, 3, 5, 4))
-    segments((2, 0), (3, 0))
-    segments((2, 1), (3, 1))
     kv_waits(2)
-    segments((2, 2), (3, 2))
+    segments((0, 2), (1, 2))
     kv_waits(3)
-    segments((2, 3), (3, 3))
-    for j in (4, 5, 3, 6):
+    segments((0, 3), (1, 3))
+    own_o, own_t = finish(0)
+    for j in (3, 2, 1):
         finish(j)
-    segments((0, 2), (1, 2))
-    segments((0, 3), (1, 3))
-    for j in (2, 1, 7):
+    q_waits((7, 6))
+    segments((2, 0), (2, 1))
+    segments((2, 2), (2, 3))
+    for j in (6, 7):
         finish(j)
-    own_o, own_t = finish(0)
+    q_waits((5, 4))
+    segments((3, 0), (3, 1))
+    segments((3, 2), (3, 3))
+    for j in (4, 5):
+        finish(j)
 
     def from_owner(j, e, which):
         frm = lax.rem(z + NZ - j, NZ) * NY + (y_other if e else y)
@@ -547,6 +570,7 @@
         v((NT, cut, feats + rows), bf), v((NT, cut, feats + rows), bf), v((2, cut, feats), f32), v((cut, feats), bf),
         dma((14,)), dma, dma((8,)), dma((NT,)), dma((NY,)), dma((NY,)), dma((NZ, 2)), dma((NZ, 2)), dma, dma,
         dma((NZ, 2)), dma((NZ, 2)), dma((NZ, 2)), dma((NZ, 2)), dma((2,)), dma((2,)), dma((2, NX)), dma((2, NX)), dma((NT,)), dma((NT,)), dma,
+        pltpu.SemaphoreType.REGULAR,
     ]
     return pl.pallas_call(
         kernel,

time: 50.6 us -> 46.3 us (0.915)
  the two profiles are of different devices: /device:TPU:1 before, /device:TPU:256 now
where the time goes in v6:
time: 46.3 us; the launch traced here: 46.1 us
  Pallas kernels  44.6 us (96%)
  local copies, waits for them, and re-layouts  1.47 us (3%)
    pallas_call x1, Pallas kernels, one_kernel(): pl.pallas_call(kernel, out_shape=jax.ShapeDtypeStruct((cut, feats), bf),...  44.6 us
    unnamed x1, local copies, waits for them, and re-layouts  1.47 us

profile of v6, /device:TPU:256, one launch (start us, length us, event | category | flops | bytes accessed | tf_op | source)
XLA Modules:
  0.0 46.1 jit_solution(9367851466145242103)
XLA Ops:
  0.0 44.6 %layer.1 = bf16[16,2048]{1,0:T(8,128)(2,1)} custom-call(bf16[128,256]{1,0:T(8,128)(2,1)} %tokens.1, f32[2048]{0:T(1024)} %pre_gain_in.1, bf16[2048,128]{1,0:T(8,128)(2,1)} %wqs.1, bf16[2048,128]{1,0:T(8,128)(2,1)} %wks.1, bf16[2048,128]{1,0:T(8,128)(2,1)} %wvs.1, bf16[2048,128]{1,0:T(8,128)(2,1)} %wqw.1, bf16[64,2048]{1,0:T(8,128)(2,1)} %bitcast.2, ...), custom_call_target="tpu_custom_call" | custom-call | tf_op jit(solution)/shard_map/layer/pallas_call | solution.py:575
  44.6 1.5 %copy.17 = bf16[16,2048]{1,0:T(8,128)(2,1)} copy(bf16[16,2048]{1,0:T(8,128)(2,1)} %layer.1) | data formatting | bytes 131072

commit v7 on v6

--- a/solution.py
+++ b/solution.py
@@ -174,9 +174,6 @@
     def kv_send(k):
         start(kv_copy(kv_other if k % 2 else kv_all.at[y], y, k, lax.rem(y + k, NY)))
 
-    for k in (1, 7):
-        kv_send(k)
-
     qs = proj[:, 2 * rows : 3 * rows] * inv
     q0 = jnp.where(left_half, qs[:half], pltpu.roll(qs[half:], hd, 1))
     q1 = jnp.where(left_half, pltpu.roll(qs[:half], hd, 1), qs[half:])
@@ -184,17 +181,24 @@
     q_other[...] = jnp.where(head == 0, q1, q0).astype(bf)
 
     def q_copy(j, e, to_z):
-        src = q_other if e else q_all.at[0, 0]
-        return remote(
-            src, q_all.at[PLACE[j], e], q_ss.at[j, e], q_rs.at[j, e], to_z * NY + (y_other if e else y), t
-        )
+        src = q_all.at[0, e] if j > 1 or e == 0 else q_other
+        to_y = y_other if e and j < 2 else y
+        return remote(src, q_all.at[PLACE[j], e], q_ss.at[j, e], q_rs.at[j, e], to_z * NY + to_y, t)
+
+    def q_send(e, *js):
+        for j in js:
+            @pl.when(z - j >= 0)
+            def _():
+                q_copy(j, e, z - j).start()
 
     start(q_copy(0, 1, z))
-    for j in (1, 7, 2, 6, 3, 5, 4):
-        @pl.when(z - j >= 0)
-        def _():
-            q_copy(j, 0, z - j).start()
-            q_copy(j, 1, z - j).start()
+    q_send(0, 1)
+    q_send(1, 1)
+    for k in (1, 7):
+        kv_send(k)
+    q_send(0, 4, 5, 3)
+    kv_send(4)
+    q_send(0, 2, 6, 7)
 
     kvw[...] = (kvw_acc[...] * inv).astype(bf)
 
@@ -205,7 +209,7 @@
     def _():
         prev_copy(s + 1).start()
 
-    for k in (2, 6, 3, 5, 4):
+    for k in (3, 5, 2, 6):
         kv_send(k)
 
     @pl.when(ends_row)
@@ -283,8 +287,7 @@
         for j in js:
             @pl.when(z + j < NZ)
             def _():
-                if j:
-                    q_wait(j, 0)
+                q_wait(j, 0)
                 q_wait(j, 1)
 
     kt = 2 * rows
@@ -397,31 +400,28 @@
     def segments(*pairs):
         segment(pairs)
 
-    q_waits((0, 1))
+    q_wait(0, 1)
+    q_send(1, 4, 5, 3, 2, 6, 7)
+    q_waits((1,))
     kv_waits(0)
     segments((0, 0))
     windowed()
     kv_waits(1)
-    q_waits((2, 3))
-    segments((0, 1), (1, 1))
-    segments((1, 0))
+    segments((0, 1))
     kv_waits(2)
-    segments((0, 2), (1, 2))
     kv_waits(3)
-    segments((0, 3), (1, 3))
+    segments((0, 2), (0, 3))
     own_o, own_t = finish(0)
-    for j in (3, 2, 1):
-        finish(j)
-    q_waits((7, 6))
-    segments((2, 0), (2, 1))
-    segments((2, 2), (2, 3))
-    for j in (6, 7):
-        finish(j)
-    q_waits((5, 4))
-    segments((3, 0), (3, 1))
-    segments((3, 2), (3, 3))
-    for j in (4, 5):
-        finish(j)
+    finish(1)
+
+    for m, js in ((1, (3, 2)), (3, (4, 5)), (2, (6, 7))):
+        @pl.when(z + min(js) < NZ)
+        def _():
+            q_waits(js)
+            segments((m, 0), (m, 1))
+            segments((m, 2), (m, 3))
+            for j in js:
+                finish(j)
 
     def from_owner(j, e, which):
         frm = lax.rem(z + NZ - j, NZ) * NY + (y_other if e else y)

time: 46.3 us -> 43.7 us (0.944)
  the two profiles are of different devices: /device:TPU:256 before, /device:TPU:320 now
where the time goes in v7:
time: 43.7 us; the launch traced here: 43.5 us
  Pallas kernels  42 us (96%)
  local copies, waits for them, and re-layouts  1.47 us (3%)
    pallas_call x1, Pallas kernels, one_kernel(): pl.pallas_call(kernel, out_shape=jax.ShapeDtypeStruct((cut, feats), bf),...  42 us
    unnamed x1, local copies, waits for them, and re-layouts  1.47 us

profile of v7, /device:TPU:320, one launch (start us, length us, event | category | flops | bytes accessed | tf_op | source)
XLA Modules:
  0.0 43.5 jit_solution(13392353085005712973)
XLA Ops:
  0.0 42.0 %layer.1 = bf16[16,2048]{1,0:T(8,128)(2,1)} custom-call(bf16[128,256]{1,0:T(8,128)(2,1)} %tokens.1, f32[2048]{0:T(1024)} %pre_gain_in.1, bf16[2048,128]{1,0:T(8,128)(2,1)} %wqs.1, bf16[2048,128]{1,0:T(8,128)(2,1)} %wks.1, bf16[2048,128]{1,0:T(8,128)(2,1)} %wvs.1, bf16[2048,128]{1,0:T(8,128)(2,1)} %wqw.1, bf16[64,2048]{1,0:T(8,128)(2,1)} %bitcast.2, ...), custom_call_target="tpu_custom_call" | custom-call | tf_op jit(solution)/shard_map/layer/pallas_call | solution.py:575
  42.0 1.5 %copy.17 = bf16[16,2048]{1,0:T(8,128)(2,1)} copy(bf16[16,2048]{1,0:T(8,128)(2,1)} %layer.1) | data formatting | bytes 131072

commit v8 on v7

--- a/solution.py
+++ b/solution.py
@@ -32,10 +32,10 @@
     tokens, pre_gain_in, wqs, wks, wvs, wqw, wkw, wvw, bias_in, sinks_in, sgain_in, wgain_in, wos, wow,
     post_gain_in, out,
     pre_gain, bias, sinks, sgain, wgain, post_gain, x, sq_acc, proj, vproj, kvw_acc, vkvw, vos, vow,
-    kv_all, kv_other, q_all, q_other, o_seg, t_seg, kvw, qw_buf, kvw_prev, o_send, o_recv, t_send, t_recv,
+    kv_all, kv_other, q_all, q_other, o_seg, t_seg, kvw, qw_buf, kvw_prev, o_send, o_recv,
     a_keep0, a_keep1, d_send0, d_send1, d_recv0, d_recv1, r_send0, r_send1, r_recv0, r_recv1,
     b_send, b_recv, total, out_buf,
-    w_sem, tok_sem, x_ss, x_rs, kv_ss, kv_rs, q_ss, q_rs, p_ss, p_rs, o_ss, o_rs, t_ss, t_rs,
+    w_sem, tok_sem, x_ss, x_rs, kv_ss, kv_rs, q_ss, q_rs, p_ss, p_rs, o_ss, o_rs,
     d_ss, d_rs, r_ss, r_rs, b_ss, b_rs, out_sem, ready,
 ):
     bf = jnp.bfloat16
@@ -100,8 +100,7 @@
 
         @pl.when(z - j < 0)
         def _():
-            o_recv[j] = jnp.zeros((2, half, rows), bf)
-            t_recv[j] = jnp.zeros((2, 8, rows), f32)
+            o_recv[j] = jnp.zeros((2, half + 8, rows), bf)
 
     for load in l_small:
         load.wait()
@@ -367,12 +366,11 @@
             def _():
                 kv_copy(kv_other, src, 0, lax.rem(y + 1, NY)).wait_recv()
 
-    def to_owner(j, e, sp, which):
-        if which:
-            return remote(o_send.at[j, e], o_recv.at[j, e], o_ss.at[j, e], o_rs.at[j, e], sp, t)
-        return remote(t_send.at[j], t_recv.at[j, e], t_ss.at[j, e], t_rs.at[j, e], sp, t)
-
-    first = lax.broadcasted_iota(jnp.int32, (8, rows), 0) < 4
+    def to_owner(j, e, sp):
+        return remote(o_send.at[j, e], o_recv.at[j, e], o_ss.at[j, e], o_rs.at[j, e], sp, t)
+
+    sublane = lax.broadcasted_iota(jnp.int32, (8, rows), 0)
+    first = sublane < 4
 
     def finish(j):
         part = slice(PLACE[j] * rows, (PLACE[j] + 1) * rows)
@@ -384,17 +382,18 @@
             carry = carry + t_seg[n, part]
         over = carry.T
         compact = jnp.where(first, over[0:8], over[hd : hd + 8])
-        o_send[j] = acc.astype(bf).reshape(2, half, rows)
-        t_send[j] = compact
+        high = compact.astype(bf).astype(f32)
+        parted = jnp.where(lax.rem(sublane, 4) < 2, high, compact - high).astype(bf)
+        for e in range(2):
+            o_send[j, e, :half] = acc[e * half : (e + 1) * half].astype(bf)
+            o_send[j, e, half:] = parted
         if j == 0:
-            for which in range(2):
-                start(to_owner(0, 1, z * NY + y_other, which))
+            start(to_owner(0, 1, z * NY + y_other))
         else:
             @pl.when(z + j < NZ)
             def _():
                 for e in range(2):
-                    for which in range(2):
-                        to_owner(j, e, (z + j) * NY + (y_other if e else y), which).start()
+                    to_owner(j, e, (z + j) * NY + (y_other if e else y)).start()
         return acc[:half], compact
 
     def segments(*pairs):
@@ -407,10 +406,9 @@
     segments((0, 0))
     windowed()
     kv_waits(1)
-    segments((0, 1))
     kv_waits(2)
     kv_waits(3)
-    segments((0, 2), (0, 3))
+    segments((0, 1), (0, 2), (0, 3))
     own_o, own_t = finish(0)
     finish(1)
 
@@ -418,36 +416,36 @@
         @pl.when(z + min(js) < NZ)
         def _():
             q_waits(js)
-            segments((m, 0), (m, 1))
-            segments((m, 2), (m, 3))
+            segments(*((m, k) for k in range(NY // 2)))
             for j in js:
                 finish(j)
 
-    def from_owner(j, e, which):
+    def from_owner(j, e):
         frm = lax.rem(z + NZ - j, NZ) * NY + (y_other if e else y)
-        to_owner(j, e, frm, which).wait_recv()
-
-    def arrivals(which):
-        from_owner(0, 1, which)
-        for j in range(1, NZ):
-            @pl.when(z - j >= 0)
-            def _():
-                from_owner(j, 0, which)
-                from_owner(j, 1, which)
-
-    arrivals(0)
+        to_owner(j, e, frm).wait_recv()
+
+    def logs_of(j, e):
+        parted = o_recv[j, e, half:].astype(f32)
+        return parted + pltpu.roll(parted, 6, 0)
+
+    from_owner(0, 1)
+    for j in range(1, NZ):
+        @pl.when(z - j >= 0)
+        def _():
+            from_owner(j, 0)
+            from_owner(j, 1)
+
     left8 = left[:8]
-    carry = jnp.where(left8, own_t, t_recv[0, 1])
+    carry = jnp.where(left8, own_t, logs_of(0, 1))
     scales = []
     for j in range(1, NZ):
         scales.append(jnp.exp2(-carry))
-        carry = carry + jnp.where(left8, t_recv[j, 0], t_recv[j, 1])
+        carry = carry + jnp.where(left8, logs_of(j, 0), logs_of(j, 1))
     scales = jnp.concatenate(scales + [jnp.zeros((rows - 8 * (NZ - 1), rows), f32)], axis=0).T
-    arrivals(1)
-    acc = jnp.concatenate([own_o, o_recv[0, 1].astype(f32)], axis=0)
+    acc = jnp.concatenate([own_o, o_recv[0, 1, :half].astype(f32)], axis=0)
     for j in range(1, NZ):
         at = 8 * (j - 1)
-        here = o_recv[j].reshape(rows, rows).astype(f32)
+        here = jnp.concatenate([o_recv[j, 0, :half].astype(f32), o_recv[j, 1, :half].astype(f32)], axis=0)
         acc = acc + jnp.where(left, scales[:, at : at + 1], scales[:, at + 4 : at + 5]) * here
     head0 = jnp.where(head == 0, acc[:half], acc[half:])
     head1 = jnp.where(head == 0, acc[half:], acc[:half])
@@ -533,8 +531,7 @@
 
             @pl.when(z + j < NZ)
             def _():
-                for which in range(2):
-                    to_owner(j, e, (z + j) * NY + (y_other if e else y), which).wait_send()
+                to_owner(j, e, (z + j) * NY + (y_other if e else y)).wait_send()
 
     @pl.when(s < N_SP - 1)
     def _():
@@ -563,13 +560,12 @@
         v((NY, rows, rows), bf), v((rows, rows), bf), v((NZ, 2, rows // 2, rows), bf), v((rows // 2, rows), bf),
         v((NY // 2, NZ * rows, rows), f32), v((NY // 2, NZ * rows, rows), f32),
         v((rows, rows), bf), v((rows, rows), f32), v((rows, rows), bf),
-        v((NZ, 2, rows // 2, rows), bf), v((NZ, 2, rows // 2, rows), bf),
-        v((NZ, 8, rows), f32), v((NZ, 2, 8, rows), f32),
+        v((NZ, 2, rows // 2 + 8, rows), bf), v((NZ, 2, rows // 2 + 8, rows), bf),
         *(v((NX, cut, width), f32) for width in widths),
         *(v((NX, cut, width), bf) for _ in range(4) for width in widths),
         v((NT, cut, feats + rows), bf), v((NT, cut, feats + rows), bf), v((2, cut, feats), f32), v((cut, feats), bf),
         dma((14,)), dma, dma((8,)), dma((NT,)), dma((NY,)), dma((NY,)), dma((NZ, 2)), dma((NZ, 2)), dma, dma,
-        dma((NZ, 2)), dma((NZ, 2)), dma((NZ, 2)), dma((NZ, 2)), dma((2,)), dma((2,)), dma((2, NX)), dma((2, NX)), dma((NT,)), dma((NT,)), dma,
+        dma((NZ, 2)), dma((NZ, 2)), dma((2,)), dma((2,)), dma((2, NX)), dma((2, NX)), dma((NT,)), dma((NT,)), dma,
         pltpu.SemaphoreType.REGULAR,
     ]
     return pl.pallas_call(

time: 43.7 us -> 42.9 us (0.982)
  the two profiles are of different devices: /device:TPU:320 before, /device:TPU:1 now
where the time goes in v8:
time: 42.9 us; the launch traced here: 42.3 us
  Pallas kernels  40.8 us (95%)
  local copies, waits for them, and re-layouts  1.47 us (3%)
    pallas_call x1, Pallas kernels, one_kernel(): pl.pallas_call(kernel, out_shape=jax.ShapeDtypeStruct((cut, feats), bf),...  40.8 us
    unnamed x1, local copies, waits for them, and re-layouts  1.47 us

profile of v8, /device:TPU:1, one launch (start us, length us, event | category | flops | bytes accessed | tf_op | source)
XLA Modules:
  0.0 42.3 jit_solution(8764554738503216595)
XLA Ops:
  0.0 40.8 %layer.1 = bf16[16,2048]{1,0:T(8,128)(2,1)} custom-call(bf16[128,256]{1,0:T(8,128)(2,1)} %tokens.1, f32[2048]{0:T(1024)} %pre_gain_in.1, bf16[2048,128]{1,0:T(8,128)(2,1)} %wqs.1, bf16[2048,128]{1,0:T(8,128)(2,1)} %wks.1, bf16[2048,128]{1,0:T(8,128)(2,1)} %wvs.1, bf16[2048,128]{1,0:T(8,128)(2,1)} %wqw.1, bf16[64,2048]{1,0:T(8,128)(2,1)} %bitcast.2, ...), custom_call_target="tpu_custom_call" | custom-call | tf_op jit(solution)/shard_map/layer/pallas_call | solution.py:571
  40.8 1.5 %copy.17 = bf16[16,2048]{1,0:T(8,128)(2,1)} copy(bf16[16,2048]{1,0:T(8,128)(2,1)} %layer.1) | data formatting | bytes 131072

commit v9 on v8

--- a/solution.py
+++ b/solution.py
@@ -155,7 +155,8 @@
         load.wait()
     absorb(t, block(0, 1), first=True)
     absorb(*[block(dx, 0) for dx in (1, 3, 2)])
-    absorb(*[block(dx, 1) for dx in (1, 3, 2)])
+    absorb(*[block(dx, 1) for dx in (1, 3)])
+    absorb(block(2, 1))
     inv = lax.rsqrt(jnp.sum(sq_acc[...], axis=1, keepdims=True) * (1.0 / feats) + EPS)
 
     left = lax.broadcasted_iota(jnp.int32, (rows, rows), 1) < hd
@@ -515,7 +516,7 @@
     inv_s = lax.rsqrt(sums[:, :1] * (1.0 / (NT * rows)) + EPS)
     both = (total[0] * inv_s + total[1]).astype(bf).astype(f32)
     stats = jnp.sum(both * both, axis=1, keepdims=True) * (1.0 / feats)
-    out_buf[...] = (both * lax.rsqrt(stats + EPS) * post_gain[...].reshape(1, feats)).astype(bf)
+    out_buf[...] = both * lax.rsqrt(stats + EPS)
 
     out_copy = pltpu.make_async_copy(out_buf, out, out_sem)
     out_copy.start()
@@ -563,14 +564,14 @@
         v((NZ, 2, rows // 2 + 8, rows), bf), v((NZ, 2, rows // 2 + 8, rows), bf),
         *(v((NX, cut, width), f32) for width in widths),
         *(v((NX, cut, width), bf) for _ in range(4) for width in widths),
-        v((NT, cut, feats + rows), bf), v((NT, cut, feats + rows), bf), v((2, cut, feats), f32), v((cut, feats), bf),
+        v((NT, cut, feats + rows), bf), v((NT, cut, feats + rows), bf), v((2, cut, feats), f32), v((cut, feats), f32),
         dma((14,)), dma, dma((8,)), dma((NT,)), dma((NY,)), dma((NY,)), dma((NZ, 2)), dma((NZ, 2)), dma, dma,
         dma((NZ, 2)), dma((NZ, 2)), dma((2,)), dma((2,)), dma((2, NX)), dma((2, NX)), dma((NT,)), dma((NT,)), dma,
         pltpu.SemaphoreType.REGULAR,
     ]
-    return pl.pallas_call(
+    normed = pl.pallas_call(
         kernel,
-        out_shape=jax.ShapeDtypeStruct((cut, feats), bf),
+        out_shape=jax.ShapeDtypeStruct((cut, feats), f32),
         in_specs=[anywhere] * len(args),
         out_specs=anywhere,
         scratch_shapes=scratch,
@@ -579,6 +580,7 @@
         ),
         name="layer",
     )(*args[:6], wkw.T, wvw.T, *args[8:])
+    return (normed * post_gain.reshape(1, feats)).astype(bf)
 
 
 def solution(mesh):

time: 42.9 us -> 43.1 us (level)
  other arithmetic: 0 us -> 1.55 us
  local copies, waits for them, and re-layouts: 1.47 us -> 0 us
    convert_element_type x0 -> x1, other arithmetic: none -> 1.55 us  [one_kernel(): return (normed * post_gain.reshape(1, feats)).astype(bf)]
    unnamed x1 -> x0, local copies, waits for them, and re-layouts: 1.47 us -> none
where the time goes in v9:
time: 43.1 us; the launch traced here: 42.4 us
  Pallas kernels  40.8 us (95%)
  other arithmetic  1.55 us (4%)
    pallas_call x1, Pallas kernels, one_kernel(): pl.pallas_call(kernel, out_shape=jax.ShapeDtypeStruct((cut, feats), f32),...  40.8 us
    convert_element_type x1, other arithmetic, one_kernel(): return (normed * post_gain.reshape(1, feats)).astype(bf)  1.55 us

profile of v9, /device:TPU:1, one launch (start us, length us, event | category | flops | bytes accessed | tf_op | source)
XLA Modules:
  0.0 42.4 jit_solution(6577147816206801115)
XLA Ops:
  0.0 40.8 %layer.1 = f32[16,2048]{1,0:T(8,128)} custom-call(bf16[128,256]{1,0:T(8,128)(2,1)} %tokens.1, f32[2048]{0:T(1024)} %pre_gain_in.1, bf16[2048,128]{1,0:T(8,128)(2,1)} %wqs.1, bf16[2048,128]{1,0:T(8,128)(2,1)} %wks.1, bf16[2048,128]{1,0:T(8,128)(2,1)} %wvs.1, bf16[2048,128]{1,0:T(8,128)(2,1)} %wqw.1, bf16[64,2048]{1,0:T(8,128)(2,1)} %bitcast.2, ...), custom_call_target="tpu_custom_call" | custom-call | tf_op jit(solution)/shard_map/layer/pallas_call | solution.py:572
  40.9 1.5 %multiply_convert_fusion = bf16[16,2048]{1,0:T(8,128)(2,1)} fusion(f32[16,2048]{1,0:T(8,128)} %layer.1, f32[2048]{0:T(1024)} %post_gain_in.1), kind=kLoop, calls=%fused_computation | loop fusion | flops 65536 | bytes 204800 | tf_op jit(solution)/shard_map/convert_element_type | solution.py:583
